TPU v7x, 32 devices: a whole 2x2x4 slice. The times are simulated.
32 devices in a mesh: sp: 8 (over z, y), tp: 4 (over x, core).
Axes of the slice: x: 2, y: 2, z: 4, core: 2. Of those that a mesh axis runs over, the one named last changes fastest.
Arguments:
- resid: bfloat16 [8192, 2048], P(('sp', 'tp')), may hold values from -6 to 6
- queries: bfloat16 [8192, 2048], P('sp', 'tp'), may hold values from -6 to 6
- keys: bfloat16 [8192, 2048], P('sp', 'tp'), may hold values from -6 to 6
- values: bfloat16 [8192, 4096], P('sp', 'tp'), may hold values from -6 to 6
- gates: bfloat16 [8192, 4096], P('sp', 'tp'), may hold values from -6 to 6
- log_decay: float32 [8, 8192], P('tp', 'sp'), may hold values from -1 to 0
- retention_output_weight: bfloat16 [4096, 2048], P('tp'), may hold values from -0.125 to 0.125
- norm_gain: bfloat16 [2048], replicated, may hold values from 0.099609375 to 1.8984375
- up_weight: bfloat16 [2048, 8192], P('sp', 'tp'), may hold values from -0.125 to 0.125
- down_weight: bfloat16 [8192, 2048], P('tp', 'sp'), may hold values from -0.0625 to 0.0625
Outputs:
- layer_out: bfloat16 [8192, 2048], P(('sp', 'tp'))
All inputs are finite; a program needn't handle non-finite values.
Results may differ from a plain program's by a relative error of at most 0.02.
Values may be sent and summed in bfloat16 or wider, within the bound.
A program may use at most 128 MiB of HBM per device.

v0:
```python
import functools

import jax
import jax.numpy as jnp
import numpy as np
from jax import lax
from jax.experimental import pallas as pl
from jax.experimental.pallas import tpu as pltpu
from jax.sharding import PartitionSpec as P

DK = 256
DV = 512
BLOCK = 128
SPAN = 256
ROWS = 4
EPS = 1e-06
F32 = jnp.float32
BF16 = jnp.bfloat16
MESH = pl.DeviceIdType.MESH


def dot(a, b):
    return jnp.dot(a, b, preferred_element_type=F32)


def cumulative(row):
    n = row.shape[1]
    i = lax.broadcasted_iota(jnp.int32, (n, n), 0)
    j = lax.broadcasted_iota(jnp.int32, (n, n), 1)
    col = jnp.sum(jnp.where(i == j, row, 0.0), axis=1, keepdims=True)
    cum_col = jnp.sum(jnp.where(j <= i, row, 0.0), axis=1, keepdims=True)
    cum_row = jnp.sum(jnp.where(i <= j, col, 0.0), axis=0, keepdims=True)
    total = jnp.sum(row, axis=1, keepdims=True)
    return i, j, cum_col, cum_row, total


def kernel(
    n_sp, n_tp,
    resid_h, q_h, k_h, v_h, g_h, ld, wo_h, gain, up_h, dn_h, lo_c, lo_s, hi_c, hi_s,
    out,
    q_v, k_v, v_v, g_v, wide, res_v, kr, kd, stf, sth, strun, yst, tot, ytot, crecv, csend, esend, inc, ret,
    pp, pr, psum, xr, acc, upd, x_all, up_all, dn_all, pd, qs, r1, r2y, r2x, r3y, r3x,
    lsem, wsend, wrecv, wysend, wyrecv, ssend, srecv, psend, precv, xsend, xrecv,
    asend, arx, ary, ard, rsend, rrecv,
):
    Z, X = n_sp // 2, n_tp // 2
    sp, tp = lax.axis_index("sp"), lax.axis_index("tp")
    z, y = sp // 2, sp % 2
    x, c = tp // 2, tp % 2
    rows = k_v.shape[0]
    heads = kr.shape[0]
    mine = res_v.shape[0]
    d = res_v.shape[1]
    half = up_all.shape[2]
    cols = dn_all.shape[2]
    nblk, nspan = rows // BLOCK, rows // SPAN
    rc = mine // ROWS
    has_up, has_dn = z < Z - 1, z > 0

    def rcopy(src, dst, ss, rs, dev):
        return pltpu.make_async_remote_copy(src, dst, ss, rs, device_id=dev, device_id_type=MESH)

    to_zp, to_zm = {"sp": sp + 2}, {"sp": sp - 2}
    to_y = {"sp": z * 2 + (1 - y)}
    to_c = {"tp": x * 2 + (1 - c)}

    def xat(j):
        return lax.rem(x + j + X, X)

    def to_x(j):
        return {"tp": xat(j) * 2 + c}

    pending = []

    def send(src, dst, ss, rs, dev, cond=None):
        def go():
            rcopy(src, dst, ss, rs, dev).start()

        def end():
            rcopy(src, dst, ss, rs, dev).wait_send()

        if cond is None:
            go()
        else:
            pl.when(cond)(go)
        pending.append((cond, end))

    def recv(dst, ss, rs):
        rcopy(dst, dst, ss, rs, to_c).wait_recv()

    loads = [
        (k_h, k_v), (v_h, v_v), (q_h, q_v), (g_h, g_v), (resid_h, res_v),
        (up_h.at[:, pl.ds(pl.multiple_of(y * half, half), half)], up_all.at[sp]),
        (dn_h.at[pl.ds(pl.multiple_of(y * half, half), half), :], dn_all.at[sp]),
    ]
    hv = v_v.shape[1]
    stack = wide.shape[0] // hv
    wc = d // stack
    loads += [(wo_h.at[:, pl.ds(i * wc, wc)], wide.at[pl.ds(i * hv, hv)]) for i in range(stack)]

    def load(i):
        return pltpu.make_async_copy(loads[i][0], loads[i][1], lsem.at[i])

    for i in range(len(loads)):
        load(i).start()

    barrier = pltpu.get_barrier_semaphore()
    greet = [(to_y, None), (to_c, None)] + [(to_x(j), None) for j in range(1, X)]
    greet += [(to_zp, has_up), (to_zm, has_dn)]
    for dev, cond in greet:
        def hello(dev=dev):
            pl.semaphore_signal(barrier, 1, device_id=dev, device_id_type=MESH)
        if cond is None:
            hello()
        else:
            pl.when(cond)(hello)
    pl.semaphore_wait(barrier, X + 1 + jnp.where(has_up, 1, 0) + jnp.where(has_dn, 1, 0))

    h_up = up_h.at[:, pl.ds(pl.multiple_of(y * half, half), half)]
    h_dn = dn_h.at[pl.ds(pl.multiple_of(y * half, half), half), :]
    o_up = up_h.at[:, pl.ds(pl.multiple_of((1 - y) * half, half), half)]
    o_dn = dn_h.at[pl.ds(pl.multiple_of((1 - y) * half, half), half), :]
    alls = (up_all, dn_all)

    def zsend(w, piece, src, way):
        dev, cond = ((to_zp, has_up), (to_zm, has_dn))[way]
        send(src, alls[w].at[piece], wsend.at[w, piece, way], wrecv.at[w, piece], dev, cond)

    for w, src in ((0, h_up), (1, h_dn)):
        zsend(w, sp, src, 0)
        zsend(w, sp, src, 1)
    hr = up_h.shape[0] // 2
    other = z * 2 + (1 - y)

    def ysend_up(part):
        at = pl.ds(part * hr, hr)
        send(o_up.at[at], up_all.at[sp, at], wysend.at[part], wyrecv.at[part], to_y)

    ysend_up(0)

    def fwd_y(w, ways=(0, 1), wait=True):
        if wait:
            if w == 0:
                for part in range(2):
                    at = pl.ds(part * hr, hr)
                    recv(up_all.at[other, at], wysend.at[part], wyrecv.at[part])
            else:
                recv(dn_all.at[other], wysend.at[2], wyrecv.at[2])
        for way in ways:
            zsend(w, other, alls[w].at[other], way)

    def fwd(w, k, yy):
        if k > Z - 2:
            return
        low, high = (z - k) * 2 + yy, (z + k) * 2 + yy
        for piece, way, cond in ((low, 0, (z >= k) & has_up), (high, 1, (z + k < Z) & has_dn)):
            dev = (to_zp, to_zm)[way]

            def go(piece=piece, way=way, dev=dev):
                recv(alls[w].at[piece], wsend.at[w, piece, way], wrecv.at[w, piece])
                rcopy(alls[w].at[piece], alls[w].at[piece], wsend.at[w, piece, way], wrecv.at[w, piece], dev).start()

            def end(piece=piece, way=way, dev=dev):
                rcopy(alls[w].at[piece], alls[w].at[piece], wsend.at[w, piece, way], wrecv.at[w, piece], dev).wait_send()

            pl.when(cond)(go)
            pending.append((cond, end))

    def settle(w, piece):
        plane = piece // 2
        cond = ((plane < z) & jnp.logical_not(has_up)) | ((plane > z) & jnp.logical_not(has_dn))

        @pl.when(cond)
        def _():
            recv(alls[w].at[piece], wsend.at[w, piece, 0], wrecv.at[w, piece])

    def angles(b):
        at = sp * nblk + b
        hc, hs = hi_c[pl.ds(at, 1), :], hi_s[pl.ds(at, 1), :]
        lc, ls = lo_c[...], lo_s[...]
        return hc * lc - hs * ls, hs * lc + hc * ls

    def rotated(blk, co, si):
        a, b = blk[:, : DK // 2].astype(F32), blk[:, DK // 2 :].astype(F32)
        return jnp.concatenate([a * co - b * si, a * si + b * co], axis=1)

    tot[...] = jnp.zeros_like(tot)
    load(0).wait()
    for h in range(heads):
        def state_block(t, after, h=h):
            b = nblk - 1 - t
            at = pl.ds(pl.multiple_of(b * BLOCK, BLOCK), BLOCK)
            row = ld[h : h + 1, pl.ds(pl.multiple_of(b * BLOCK, BLOCK), BLOCK)]
            i, j, cum_col, _, total = cumulative(row)
            co, si = angles(b)
            key = (rotated(k_v[at, h * DK : (h + 1) * DK], co, si) * DK ** (-0.5)).astype(BF16)
            kr[h, at, :] = key
            kd[at, :] = (key.astype(F32) * jnp.exp(total - cum_col + after)).astype(BF16)
            return after + total

        whole = lax.fori_loop(0, nblk, state_block, jnp.zeros((1, 1), F32))
        tot[h : h + 1, :] = jnp.broadcast_to(jnp.exp(whole), (1, tot.shape[1]))
        if h == 0:
            load(1).wait()
        s = lax.dot_general(kd[...], v_v[:, h * DV : (h + 1) * DV], (((0,), (0,)), ((), ())), preferred_element_type=F32)
        for p in range(2):
            part = s[:, p * DV // 2 : (p + 1) * DV // 2]
            stf[p, h] = part
            sth[p, h] = part.astype(BF16)
        send(sth.at[1 - y, h], yst.at[h], ssend.at[0, h], srecv.at[0, h], to_y)
    send(tot, ytot, ssend.at[3, 0], srecv.at[3, 0], to_y)
    ysend_up(1)
    send(o_dn, dn_all.at[sp], wysend.at[2], wyrecv.at[2], to_y)

    load(2).wait()

    def local(h):
        strun[...] = jnp.zeros_like(strun)

        def span(t, before):
            at = pl.ds(pl.multiple_of(t * SPAN, SPAN), SPAN)
            row = ld[h : h + 1, pl.ds(pl.multiple_of(t * SPAN, SPAN), SPAN)]
            i, j, cum_col, cum_row, total = cumulative(row)
            parts = []
            for u in range(SPAN // BLOCK):
                co, si = angles(t * (SPAN // BLOCK) + u)
                qat = pl.ds(pl.multiple_of(t * SPAN + u * BLOCK, BLOCK), BLOCK)
                parts.append(rotated(q_v[qat, h * DK : (h + 1) * DK], co, si))
            query = jnp.concatenate(parts, axis=0).astype(BF16)
            key = kr[h, at, :]
            factor = jnp.where(i >= j, jnp.exp(jnp.minimum(cum_col - cum_row, 0.0)), 0.0)
            scores = lax.dot_general(query, key, (((1,), (1,)), ((), ())), preferred_element_type=F32)
            weights = (scores * factor).astype(BF16)
            q32 = query.astype(F32)
            val = v_v[at, h * DV : (h + 1) * DV]
            ret[at, h * DV : (h + 1) * DV] = dot(weights, val) + dot((q32 * jnp.exp(cum_col)).astype(BF16), strun[...].astype(BF16))
            q_v[at, h * DK : (h + 1) * DK] = (q32 * jnp.exp(cum_col + before)).astype(BF16)
            kdec = (key.astype(F32) * jnp.exp(total - cum_col)).astype(BF16)
            strun[...] = jnp.exp(total) * strun[...] + lax.dot_general(
                kdec, val, (((0,), (0,)), ((), ())), preferred_element_type=F32
            )
            return before + total

        lax.fori_loop(0, nspan, span, jnp.zeros((1, 1), F32))

    local(0)

    first = y == 0
    recv(ytot, ssend.at[3, 0], srecv.at[3, 0])

    def decays(h):
        own, oth = tot[h : h + 1, : DV // 2], ytot[h : h + 1, : DV // 2]
        return jnp.where(first, own, oth), jnp.where(first, oth, own)

    @pl.when(jnp.logical_not(has_dn))
    def _():
        crecv[...] = jnp.zeros_like(crecv)

    def combine(h):
        recv(yst.at[h], ssend.at[0, h], srecv.at[0, h])

    def s_pair(h):
        own, oth = stf[y, h], yst[h].astype(F32)
        return jnp.where(first, own, oth), jnp.where(first, oth, own)

    def chain(h):
        d0, d1 = decays(h)
        s0, s1 = s_pair(h)
        csend[h] = (d0 * d1 * crecv[h].astype(F32) + (d1 * s0 + s1)).astype(BF16)

    def chain_send(h):
        rcopy(csend.at[h], crecv.at[h], ssend.at[1, h], srecv.at[1, h], to_zp).start()

    for h in range(heads):
        combine(h)
    @pl.when(jnp.logical_not(has_dn))
    def _():
        for h in range(heads):
            chain(h)
            chain_send(h)

    fwd_y(0, ways=(1,))
    late = z >= 2

    def ou_up():
        rcopy(up_all.at[other], up_all.at[other], wsend.at[0, other, 0], wrecv.at[0, other], to_zp).start()

    pl.when(late & has_up)(ou_up)
    for h in range(1, heads):
        local(h)

    @pl.when(has_dn)
    def _():
        for h in range(heads):
            recv(crecv.at[h], ssend.at[1, h], srecv.at[1, h])

            @pl.when(has_up)
            def _():
                chain(h)
                chain_send(h)

    pl.when(jnp.logical_not(late) & has_up)(ou_up)

    def chain_end():
        for h in range(heads):
            rcopy(csend.at[h], crecv.at[h], ssend.at[1, h], srecv.at[1, h], to_zp).wait_send()
        rcopy(up_all.at[other], up_all.at[other], wsend.at[0, other, 0], wrecv.at[0, other], to_zp).wait_send()

    pending.append((has_up, chain_end))
    for h in range(heads):
        d0, _ = decays(h)
        s0, _ = s_pair(h)
        got = crecv[h].astype(F32)
        later = (d0 * got + s0).astype(BF16)
        inc[y, h] = jnp.where(first, crecv[h], later)
        esend[h] = jnp.where(first, later, crecv[h])
        send(esend.at[h], inc.at[y, h], ssend.at[2, h], srecv.at[2, h], to_y)
    fwd(0, 1, y)
    fwd_y(1)
    load(3).wait()
    for i in range(stack):
        load(7 + i).wait()
    for h in range(heads):
        recv(inc.at[1 - y, h], ssend.at[2, h], srecv.at[2, h])

    fr = min(128, mine)

    def finish(owner):
        base = owner * mine

        def part(t, carry):
            at = pl.ds(pl.multiple_of(base + t * fr, fr), fr)
            for h in range(heads):
                qd = q_v[at, h * DK : (h + 1) * DK]
                r = ret[at, h * DV : (h + 1) * DV] + jnp.concatenate([dot(qd, inc[0, h]), dot(qd, inc[1, h])], axis=1)
                normed = r * lax.rsqrt(jnp.mean(r * r, axis=1, keepdims=True) + EPS)
                g = g_v[at, h * DV : (h + 1) * DV].astype(F32)
                g_v[at, h * DV : (h + 1) * DV] = (g / (1.0 + jnp.exp(-g)) * normed).astype(BF16)
            return carry

        lax.fori_loop(0, mine // fr, part, 0)

    pt = min(512, wc)

    def project(owner, put):
        rows_at = pl.ds(pl.multiple_of(owner * mine, mine), mine)
        for i in range(stack):
            def part(t, carry, i=i):
                at = pl.ds(pl.multiple_of(t * pt, pt), pt)
                to = pl.ds(pl.multiple_of(i * wc + t * pt, pt), pt)
                put(to, dot(g_v[rows_at, :], wide[i * hv : (i + 1) * hv, at]))
                return carry

            lax.fori_loop(0, wc // pt, part, 0)

    def for_sibling(j):
        owner = xat(j) * 2 + (1 - c)
        finish(owner)

        def put(at, val):
            pp[j, :, at] = val.astype(BF16)

        project(owner, put)
        send(pp.at[j], pr.at[j], psend.at[j], precv.at[j], to_c)

    def for_mine(j):
        owner = xat(j) * 2 + c
        finish(owner)

        def put(at, val):
            acc[:, at] = val.astype(BF16).astype(F32)

        project(owner, put)
        recv(pr.at[j], psend.at[j], precv.at[j])
        if j:
            for r in range(ROWS):
                at = pl.ds(r * rc, rc)
                psum[j - 1, at, :] = (acc[at, :] + pr[j, at, :].astype(F32)).astype(BF16)
                send(psum.at[j - 1, at], xr.at[j - 1, at], xsend.at[j - 1, r], xrecv.at[j - 1, r], to_x(j))

    for j in range(1, X):
        for_sibling(j)
        for_mine(j)
    fwd(0, 1, 1 - y)
    for_sibling(0)
    for_mine(0)
    fwd(0, 2, y)

    load(4).wait()
    for r in range(ROWS):
        at = pl.ds(r * rc, rc)
        s = acc[at, :] + pr[0, at, :].astype(F32)
        for j in range(1, X):
            recv(xr.at[j - 1, at], xsend.at[j - 1, r], xrecv.at[j - 1, r])
            s = s + xr[j - 1, at, :].astype(F32)
        u = (res_v[at, :].astype(F32) + s).astype(BF16)
        upd[at, :] = u
        u = u.astype(F32)
        u = u * lax.rsqrt(jnp.mean(u * u, axis=1, keepdims=True) + EPS)
        x_all[c, y, x, at, :] = (u * gain[...].astype(F32)).astype(BF16)
        own = x_all.at[c, y, x, at]
        send(own, own, asend.at[0, 0, r], ary.at[0, r], to_y)
        for j in range(1, X):
            send(own, own, asend.at[1, j, r], arx.at[j, r], to_x(j))
        send(own, own, asend.at[2, 0, r], ard.at[0, 0, r], to_c)

    load(5).wait()
    for k in range(1, Z - 1):
        if k == 1:
            continue
        fwd(0, k, 1 - y)
        if k > 2:
            fwd(0, k, y)

    for k in range(n_sp):
        settle(0, k)

    ht = min(512, half)

    def hid_rows(yy, xx):
        return pl.ds(pl.multiple_of((yy * X + xx) * mine, mine), mine)

    def hid_of(cc):
        return pl.ds(pl.multiple_of(cc * half, half), half)

    def hidden(yy, xx):
        def part(t, carry):
            at = pl.ds(pl.multiple_of(t * ht, ht), ht)
            w = up_all[:, :, at].reshape(d, ht)
            for cc in range(2):
                pre = jnp.maximum(dot(x_all[cc, yy, xx], w), 0.0)
                col = pl.ds(pl.multiple_of(cc * half + t * ht, ht), ht)
                wide[hid_rows(yy, xx), col] = (pre * pre).astype(BF16)
            return carry

        lax.fori_loop(0, half // ht, part, 0)

    def from_sibling(yrel, i, r):
        at = pl.ds(r * rc, rc)
        dst = x_all.at[1 - c, jnp.where(yrel == 0, y, 1 - y), xat(-i), at]
        recv(dst, asend.at[2, 0, r], ard.at[yrel, i, r])

    def pass_on(yrel, i, r):
        at = pl.ds(r * rc, rc)
        ref = x_all.at[c, (1 - y) if yrel else y, xat(-i), at]
        if yrel:
            recv(ref, asend.at[0, 0, r], ary.at[i, r])
        else:
            recv(ref, asend.at[1, i, r], arx.at[i, r])
            send(ref, ref, asend.at[0, i, r], ary.at[i, r], to_y)
        send(ref, ref, asend.at[2 + yrel, i, r], ard.at[yrel, i, r], to_c)

    for r in range(ROWS):
        from_sibling(0, 0, r)
    hidden(y, x)
    for r in range(ROWS):
        pass_on(1, 0, r)
        for j in range(1, X):
            pass_on(0, j, r)
        if r == 1:
            fwd(1, 1, 0)
            fwd(1, 1, 1)
    for r in range(ROWS):
        from_sibling(1, 0, r)
    hidden(1 - y, x)
    for k in range(2, Z - 1):
        fwd(1, k, 0)
        fwd(1, k, 1)
    for j in range(1, X):
        for r in range(ROWS):
            from_sibling(0, j, r)
        hidden(y, xat(-j))
    for j in range(1, X):
        for r in range(ROWS):
            pass_on(1, j, r)
        for r in range(ROWS):
            from_sibling(1, j, r)
        hidden(1 - y, xat(-j))

    load(6).wait()
    m = jnp.minimum(z, Z - 1 - z)
    hm = mine // 2

    def block_of(s):
        i = s // 2
        near = jnp.where(i % 2 == 1, z - (i + 1) // 2, z + i // 2)
        far = jnp.where(z <= Z - 1 - z, i, Z - 1 - i)
        return jnp.where(i <= 2 * m, near, far) * 2 + s % 2

    def to_sib(s):
        return rcopy(pd.at[s % 2], r1.at[s], rsend.at[0, s], rrecv.at[0, s], to_c)

    def a_y(s):
        return rcopy(qs.at[s % 4, 1 - y, :, 0], r2y.at[s], rsend.at[1, s], rrecv.at[1, s], to_y)

    def a_x(s, j):
        return rcopy(qs.at[s % 4, :, xat(j), 1], r2x.at[s, j - 1], rsend.at[3 + j, s], rrecv.at[3 + j, s], to_x(j))

    def b_y(s):
        return rcopy(qs.at[s % 4, 1 - y, x, 1], r3y.at[s], rsend.at[2, s], rrecv.at[2, s], to_y)

    def b_x(s, j):
        return rcopy(qs.at[s % 4, y, xat(j), 0], r3x.at[s, j - 1], rsend.at[3 + X + j, s], rrecv.at[3 + X + j, s], to_x(j))

    def step(s, carry):
        @pl.when(s < n_sp)
        def _():
            u = block_of(s)
            settle(1, u)

            @pl.when(s >= 2)
            def _():
                to_sib(s - 2).wait_send()

            w = dn_all[u]
            for yy in range(2):
                for xx in range(X):
                    pd[s % 2, yy, xx] = dot(wide[hid_rows(yy, xx), hid_of(1 - c)], w).astype(BF16).reshape(2, hm, cols)
            to_sib(s).start()
            for yy in range(2):
                for xx in range(X):
                    ret[hid_rows(yy, xx), :cols] = dot(wide[hid_rows(yy, xx), hid_of(c)], w)

        @pl.when((s >= 1) & (s <= n_sp))
        def _():
            p = s - 1
            a_y(p).wait_recv()
            qs[p % 4, y, :, 0] = (qs[p % 4, y, :, 0].astype(F32) + r2y[p].astype(F32)).astype(BF16)
            t = qs[p % 4, :, x, 1].astype(F32)
            for j in range(1, X):
                a_x(p, j).wait_recv()
                t = t + r2x[p, j - 1].astype(F32)
            qs[p % 4, :, x, 1] = t.astype(BF16)
            b_y(p).start()
            for j in range(1, X):
                b_x(p, j).start()

        @pl.when(s < n_sp)
        def _():
            to_sib(s).wait_recv()
            own = ret[: 2 * X * mine, :cols].reshape(2, X, 2, hm, cols)
            qs[s % 4] = (own.astype(BF16).astype(F32) + r1[s].astype(F32)).astype(BF16)
            a_y(s).start()
            for j in range(1, X):
                a_x(s, j).start()

        @pl.when(s >= 2)
        def _():
            p = s - 2
            u = block_of(p)
            at = pl.ds(pl.multiple_of(u * cols, cols), cols)
            t = upd[:hm, at].astype(F32) + qs[p % 4, y, x, 0].astype(F32)
            for j in range(1, X):
                b_x(p, j).wait_recv()
                t = t + r3x[p, j - 1].astype(F32)
            out[:hm, at] = t.astype(BF16)
            b_y(p).wait_recv()
            t = upd[hm:, at].astype(F32) + qs[p % 4, y, x, 1].astype(F32) + r3y[p].astype(F32)
            out[hm:, at] = t.astype(BF16)
            a_y(p).wait_send()
            b_y(p).wait_send()
            for j in range(1, X):
                a_x(p, j).wait_send()
                b_x(p, j).wait_send()

        return carry

    lax.fori_loop(0, n_sp + 2, step, 0)
    for s in (n_sp - 2, n_sp - 1):
        to_sib(s).wait_send()
    for cond, end in pending:
        if cond is None:
            end()
        else:
            pl.when(cond)(end)


def body(n_sp, n_tp, resid, queries, keys, values, gates, log_decay, w_out, gain, up, down):
    X, Z = n_tp // 2, n_sp // 2
    rows, heads = queries.shape[0], log_decay.shape[0]
    mine, d = resid.shape
    half, cols, part = up.shape[1] // 2, down.shape[1], up.shape[0]
    freq = 10000.0 ** (-np.arange(0, DK, 2, dtype=np.float64) / DK)
    low = np.arange(BLOCK)[:, None] * freq[None, :]
    high = (BLOCK * np.arange(rows * n_sp // BLOCK))[:, None] * freq[None, :]
    tables = [jnp.asarray(f(a), F32) for a in (low, high) for f in (np.cos, np.sin)]
    vm, anym = pl.BlockSpec(memory_space=pltpu.VMEM), pl.BlockSpec(memory_space=pl.ANY)
    dma = pltpu.SemaphoreType.DMA
    V = pltpu.VMEM
    hd, hv = heads * DK, heads * DV
    sq = (DK, DV // 2)
    scratch = [
        V((rows, hd), BF16), V((rows, hd), BF16), V((rows, hv), BF16), V((rows, hv), BF16),
        V((2 * X * mine, 2 * half), BF16), V((mine, d), BF16),
        V((heads, rows, DK), BF16), V((rows, DK), BF16),
        V((2, heads, *sq), F32), V((2, heads, *sq), BF16), V((DK, DV), F32),
        V((heads, *sq), BF16), V((8, DV // 2), F32), V((8, DV // 2), F32),
        V((heads, *sq), BF16), V((heads, *sq), BF16), V((heads, *sq), BF16), V((2, heads, *sq), BF16),
        V((rows, hv), F32),
        V((X, mine, d), BF16), V((X, mine, d), BF16), V((X - 1, mine, d), BF16), V((X - 1, mine, d), BF16),
        V((mine, d), F32), V((mine, d), BF16),
        V((2, 2, X, mine, d), BF16), V((n_sp, part, half), BF16), V((n_sp, half, cols), BF16),
        V((2, 2, X, 2, mine // 2, cols), BF16),
        V((4, 2, X, 2, mine // 2, cols), BF16), V((n_sp, 2, X, 2, mine // 2, cols), BF16),
        V((n_sp, X, mine // 2, cols), BF16), V((n_sp, X - 1, 2, mine // 2, cols), BF16),
        V((n_sp, mine // 2, cols), BF16), V((n_sp, X - 1, mine // 2, cols), BF16),
        dma((7 + 2 * X * mine // hv,)), dma((2, n_sp, 2)), dma((2, n_sp)), dma((3,)), dma((3,)),
        dma((4, heads)), dma((4, heads)), dma((X,)), dma((X,)), dma((X, ROWS)), dma((X, ROWS)),
        dma((4, X, ROWS)), dma((X, ROWS)), dma((X, ROWS)), dma((2, X, ROWS)),
        dma((4 + 2 * X, n_sp)), dma((4 + 2 * X, n_sp)),
    ]
    return pl.pallas_call(
        functools.partial(kernel, n_sp, n_tp),
        in_specs=[anym] * 5 + [vm, anym, vm, anym, anym] + [vm] * 4,
        out_specs=vm,
        out_shape=jax.ShapeDtypeStruct((mine, d), BF16),
        scratch_shapes=scratch,
        compiler_params=pltpu.CompilerParams(
            collective_id=0, has_side_effects=True, vmem_limit_bytes=67043328
        ),
        name="layer",
    )(resid, queries, keys, values, gates, log_decay, w_out, gain.reshape(1, d), up, down, *tables)


def solution(mesh):
    placed = (
        P(("sp", "tp"), None),
        P("sp", "tp"),
        P("sp", "tp"),
        P("sp", "tp"),
        P("sp", "tp"),
        P("tp", "sp"),
        P("tp", None),
        P(),
        P("sp", "tp"),
        P("tp", "sp"),
    )
    return jax.shard_map(
        functools.partial(body, mesh.shape["sp"], mesh.shape["tp"]),
        mesh=mesh,
        in_specs=placed,
        out_specs=P(("sp", "tp"), None),
        check_vma=False,
    )
```

profile of v0, /device:TPU:24, one launch (start us, length us, event | category | flops | bytes accessed | tf_op | source)
XLA Modules:
  0.0 186.9 jit_solution(18312371032337819866)
XLA Ops:
  0.0 1.3 reshape.3.gain
  1.3 183.3 %layer.1 = bf16[256,2048]{1,0:T(8,128)(2,1)} custom-call(bf16[256,2048]{1,0:T(8,128)(2,1)} %resid_h.1, bf16[1024,512]{1,0:T(8,128)(2,1)} %q_h.1, bf16[1024,512]{1,0:T(8,128)(2,1)} %k_h.1, bf16[1024,1024]{1,0:T(8,128)(2,1)} %v_h.1, bf16[1024,1024]{1,0:T(8,128)(2,1)} %g_h.1, f32[2,1024]{1,0:T(2,128)} %ld.1, bf16[1024,2048]{1,0:T(8,128)(2,1)} %wo_h.1, ...), custom_call_target="tpu_custom_call" | custom-call | tf_op jit(solution)/shard_map/layer/pallas_call | solution.py:612
  184.6 2.3 %copy.16 = bf16[256,2048]{1,0:T(8,128)(2,1)} copy(bf16[256,2048]{1,0:T(8,128)(2,1)} %layer.1) | data formatting | bytes 2097152
where the time goes:
time: 187 us
  Pallas kernels  183 us (98%)
  local copies, waits for them, and re-layouts  3.59 us (2%)
    pallas_call x1, Pallas kernels, body(): pl.pallas_call(functools.partial(kernel, n_sp, n_tp), in_specs=[anym] * 5...  183 us

commit v1 on v0

--- a/solution.py
+++ b/solution.py
@@ -13,6 +13,7 @@
 BLOCK = 128
 SPAN = 256
 ROWS = 4
+SLOTS = 6
 EPS = 1e-06
 F32 = jnp.float32
 BF16 = jnp.bfloat16
@@ -126,45 +127,49 @@
         dev, cond = ((to_zp, has_up), (to_zm, has_dn))[way]
         send(src, alls[w].at[piece], wsend.at[w, piece, way], wrecv.at[w, piece], dev, cond)
 
-    for w, src in ((0, h_up), (1, h_dn)):
-        zsend(w, sp, src, 0)
-        zsend(w, sp, src, 1)
+    late = z >= 2
+    early = jnp.logical_not(late)
+    for way in range(2):
+        zsend(0, sp, h_up, way)
+    zsend(1, sp, h_dn, 1)
+
+    def own_dn():
+        return rcopy(h_dn, dn_all.at[sp], wsend.at[1, sp, 0], wrecv.at[1, sp], to_zp)
+
+    @pl.when(late & has_up)
+    def _():
+        own_dn().start()
+
+    pending.append((has_up, lambda: own_dn().wait_send()))
     hr = up_h.shape[0] // 2
     other = z * 2 + (1 - y)
 
-    def ysend_up(part):
-        at = pl.ds(part * hr, hr)
-        send(o_up.at[at], up_all.at[sp, at], wysend.at[part], wyrecv.at[part], to_y)
-
-    ysend_up(0)
-
-    def fwd_y(w, ways=(0, 1), wait=True):
-        if wait:
-            if w == 0:
-                for part in range(2):
-                    at = pl.ds(part * hr, hr)
-                    recv(up_all.at[other, at], wysend.at[part], wyrecv.at[part])
-            else:
-                recv(dn_all.at[other], wysend.at[2], wyrecv.at[2])
-        for way in ways:
-            zsend(w, other, alls[w].at[other], way)
-
-    def fwd(w, k, yy):
-        if k > Z - 2:
-            return
+    def ysend(w, src):
+        send(src, alls[w].at[sp], wysend.at[w], wyrecv.at[w], to_y)
+
+    def recv_y(w):
+        recv(alls[w].at[other], wysend.at[w], wyrecv.at[w])
+
+    def relays(w, k, yy):
+        parts = []
         low, high = (z - k) * 2 + yy, (z + k) * 2 + yy
         for piece, way, cond in ((low, 0, (z >= k) & has_up), (high, 1, (z + k < Z) & has_dn)):
-            dev = (to_zp, to_zm)[way]
-
-            def go(piece=piece, way=way, dev=dev):
-                recv(alls[w].at[piece], wsend.at[w, piece, way], wrecv.at[w, piece])
-                rcopy(alls[w].at[piece], alls[w].at[piece], wsend.at[w, piece, way], wrecv.at[w, piece], dev).start()
-
-            def end(piece=piece, way=way, dev=dev):
-                rcopy(alls[w].at[piece], alls[w].at[piece], wsend.at[w, piece, way], wrecv.at[w, piece], dev).wait_send()
-
-            pl.when(cond)(go)
-            pending.append((cond, end))
+            def copy(piece=piece, way=way):
+                ref = alls[w].at[piece]
+                return rcopy(ref, ref, wsend.at[w, piece, way], wrecv.at[w, piece], (to_zp, to_zm)[way])
+
+            def go(copy=copy):
+                copy().wait_recv()
+                copy().start()
+
+            pending.append((cond, lambda copy=copy: copy().wait_send()))
+            parts.append((cond, go))
+        return parts
+
+    def fwd(w, k, yy):
+        if k <= Z - 2:
+            for cond, go in relays(w, k, yy):
+                pl.when(cond)(go)
 
     def settle(w, piece):
         plane = piece // 2
@@ -209,8 +214,8 @@
             sth[p, h] = part.astype(BF16)
         send(sth.at[1 - y, h], yst.at[h], ssend.at[0, h], srecv.at[0, h], to_y)
     send(tot, ytot, ssend.at[3, 0], srecv.at[3, 0], to_y)
-    ysend_up(1)
-    send(o_dn, dn_all.at[sp], wysend.at[2], wyrecv.at[2], to_y)
+    ysend(0, o_up)
+    ysend(1, o_dn)
 
     load(2).wait()
 
@@ -278,16 +283,19 @@
         for h in range(heads):
             chain(h)
             chain_send(h)
-
-    fwd_y(0, ways=(1,))
-    late = z >= 2
-
-    def ou_up():
-        rcopy(up_all.at[other], up_all.at[other], wsend.at[0, other, 0], wrecv.at[0, other], to_zp).start()
-
-    pl.when(late & has_up)(ou_up)
+        own_dn().start()
+
     for h in range(1, heads):
         local(h)
+
+    def part_up(part):
+        ref = up_all.at[other, pl.ds(part * hr, hr)]
+        rcopy(ref, ref, wsend.at[0, other, 0], wrecv.at[0, other], to_zp).start()
+
+    @pl.when(late)
+    def _():
+        recv_y(0)
+        pl.when(has_up)(lambda: part_up(0))
 
     @pl.when(has_dn)
     def _():
@@ -299,7 +307,9 @@
                 chain(h)
                 chain_send(h)
 
-    pl.when(jnp.logical_not(late) & has_up)(ou_up)
+        @pl.when(early & has_up)
+        def _():
+            own_dn().start()
 
     def chain_end():
         for h in range(heads):
@@ -315,18 +325,24 @@
         inc[y, h] = jnp.where(first, crecv[h], later)
         esend[h] = jnp.where(first, later, crecv[h])
         send(esend.at[h], inc.at[y, h], ssend.at[2, h], srecv.at[2, h], to_y)
+    @pl.when(early)
+    def _():
+        recv_y(0)
+        pl.when(has_up)(lambda: part_up(0))
+
+    pl.when(has_up)(lambda: part_up(1))
+    zsend(0, other, up_all.at[other], 1)
     fwd(0, 1, y)
-    fwd_y(1)
     load(3).wait()
     for i in range(stack):
         load(7 + i).wait()
     for h in range(heads):
         recv(inc.at[1 - y, h], ssend.at[2, h], srecv.at[2, h])
 
-    fr = min(128, mine)
-
-    def finish(owner):
-        base = owner * mine
+    ph = mine // 2
+    fr = min(128, ph)
+
+    def finish(base):
 
         def part(t, carry):
             at = pl.ds(pl.multiple_of(base + t * fr, fr), fr)
@@ -338,12 +354,12 @@
                 g_v[at, h * DV : (h + 1) * DV] = (g / (1.0 + jnp.exp(-g)) * normed).astype(BF16)
             return carry
 
-        lax.fori_loop(0, mine // fr, part, 0)
+        lax.fori_loop(0, ph // fr, part, 0)
 
     pt = min(512, wc)
 
-    def project(owner, put):
-        rows_at = pl.ds(pl.multiple_of(owner * mine, mine), mine)
+    def project(base, put):
+        rows_at = pl.ds(pl.multiple_of(base, ph), ph)
         for i in range(stack):
             def part(t, carry, i=i):
                 at = pl.ds(pl.multiple_of(t * pt, pt), pt)
@@ -353,37 +369,44 @@
 
             lax.fori_loop(0, wc // pt, part, 0)
 
-    def for_sibling(j):
-        owner = xat(j) * 2 + (1 - c)
-        finish(owner)
+    def for_sibling(j, p):
+        base = (xat(j) * 2 + (1 - c)) * mine + p * ph
+        finish(base)
+        mid = pl.ds(p * ph, ph)
 
         def put(at, val):
-            pp[j, :, at] = val.astype(BF16)
-
-        project(owner, put)
-        send(pp.at[j], pr.at[j], psend.at[j], precv.at[j], to_c)
-
-    def for_mine(j):
-        owner = xat(j) * 2 + c
-        finish(owner)
+            pp[j, mid, at] = val.astype(BF16)
+
+        project(base, put)
+        send(pp.at[j, mid], pr.at[j, mid], psend.at[j, p], precv.at[j, p], to_c)
+
+    def for_mine(j, p):
+        base = (xat(j) * 2 + c) * mine + p * ph
+        finish(base)
+        mid = pl.ds(p * ph, ph)
 
         def put(at, val):
-            acc[:, at] = val.astype(BF16).astype(F32)
-
-        project(owner, put)
-        recv(pr.at[j], psend.at[j], precv.at[j])
+            acc[mid, at] = val.astype(BF16).astype(F32)
+
+        project(base, put)
+        recv(pr.at[j, mid], psend.at[j, p], precv.at[j, p])
         if j:
-            for r in range(ROWS):
+            for r in range(p * ROWS // 2, (p + 1) * ROWS // 2):
                 at = pl.ds(r * rc, rc)
                 psum[j - 1, at, :] = (acc[at, :] + pr[j, at, :].astype(F32)).astype(BF16)
                 send(psum.at[j - 1, at], xr.at[j - 1, at], xsend.at[j - 1, r], xrecv.at[j - 1, r], to_x(j))
 
     for j in range(1, X):
-        for_sibling(j)
-        for_mine(j)
+        for p in range(2):
+            for_sibling(j, p)
+            for_mine(j, p)
     fwd(0, 1, 1 - y)
-    for_sibling(0)
-    for_mine(0)
+    for p in range(2):
+        for_sibling(0, p)
+        for_mine(0, p)
+    recv_y(1)
+    for way in range(2):
+        zsend(1, other, dn_all.at[other], way)
     fwd(0, 2, y)
 
     load(4).wait()
@@ -412,9 +435,6 @@
         if k > 2:
             fwd(0, k, y)
 
-    for k in range(n_sp):
-        settle(0, k)
-
     ht = min(512, half)
 
     def hid_rows(yy, xx):
@@ -451,29 +471,29 @@
         send(ref, ref, asend.at[2 + yrel, i, r], ard.at[yrel, i, r], to_c)
 
     for r in range(ROWS):
-        from_sibling(0, 0, r)
-    hidden(y, x)
+        pass_on(1, 0, r)
     for r in range(ROWS):
-        pass_on(1, 0, r)
         for j in range(1, X):
             pass_on(0, j, r)
         if r == 1:
             fwd(1, 1, 0)
-            fwd(1, 1, 1)
+    fwd(1, 1, 1)
+    for k in range(n_sp):
+        settle(0, k)
+    for r in range(ROWS):
+        from_sibling(0, 0, r)
+    hidden(y, x)
     for r in range(ROWS):
         from_sibling(1, 0, r)
     hidden(1 - y, x)
-    for k in range(2, Z - 1):
-        fwd(1, k, 0)
-        fwd(1, k, 1)
     for j in range(1, X):
+        for r in range(ROWS):
+            pass_on(1, j, r)
         for r in range(ROWS):
             from_sibling(0, j, r)
         hidden(y, xat(-j))
     for j in range(1, X):
         for r in range(ROWS):
-            pass_on(1, j, r)
-        for r in range(ROWS):
             from_sibling(1, j, r)
         hidden(1 - y, xat(-j))
 
@@ -491,18 +511,24 @@
         return rcopy(pd.at[s % 2], r1.at[s], rsend.at[0, s], rrecv.at[0, s], to_c)
 
     def a_y(s):
-        return rcopy(qs.at[s % 4, 1 - y, :, 0], r2y.at[s], rsend.at[1, s], rrecv.at[1, s], to_y)
+        return rcopy(qs.at[s % SLOTS, 1 - y, :, 0], r2y.at[s], rsend.at[1, s], rrecv.at[1, s], to_y)
 
     def a_x(s, j):
-        return rcopy(qs.at[s % 4, :, xat(j), 1], r2x.at[s, j - 1], rsend.at[3 + j, s], rrecv.at[3 + j, s], to_x(j))
+        return rcopy(qs.at[s % SLOTS, :, xat(j), 1], r2x.at[s, j - 1], rsend.at[3 + j, s], rrecv.at[3 + j, s], to_x(j))
 
     def b_y(s):
-        return rcopy(qs.at[s % 4, 1 - y, x, 1], r3y.at[s], rsend.at[2, s], rrecv.at[2, s], to_y)
+        return rcopy(qs.at[s % SLOTS, 1 - y, x, 1], r3y.at[s], rsend.at[2, s], rrecv.at[2, s], to_y)
 
     def b_x(s, j):
-        return rcopy(qs.at[s % 4, y, xat(j), 0], r3x.at[s, j - 1], rsend.at[3 + X + j, s], rrecv.at[3 + X + j, s], to_x(j))
+        return rcopy(qs.at[s % SLOTS, y, xat(j), 0], r3x.at[s, j - 1], rsend.at[3 + X + j, s], rrecv.at[3 + X + j, s], to_x(j))
+
+    last = [(2 * (k - 2 + yy), relays(1, k, yy)) for k in range(2, Z - 1) for yy in range(2)]
 
     def step(s, carry):
+        for at, parts in last:
+            for cond, go in parts:
+                pl.when(cond & (s == at))(go)
+
         @pl.when(s < n_sp)
         def _():
             u = block_of(s)
@@ -513,24 +539,20 @@
                 to_sib(s - 2).wait_send()
 
             w = dn_all[u]
-            for yy in range(2):
-                for xx in range(X):
-                    pd[s % 2, yy, xx] = dot(wide[hid_rows(yy, xx), hid_of(1 - c)], w).astype(BF16).reshape(2, hm, cols)
+            pd[s % 2] = dot(wide[:, hid_of(1 - c)], w).astype(BF16).reshape(2, X, 2, hm, cols)
             to_sib(s).start()
-            for yy in range(2):
-                for xx in range(X):
-                    ret[hid_rows(yy, xx), :cols] = dot(wide[hid_rows(yy, xx), hid_of(c)], w)
-
-        @pl.when((s >= 1) & (s <= n_sp))
+            ret[: 2 * X * mine, :cols] = dot(wide[:, hid_of(c)], w)
+
+        @pl.when((s >= 2) & (s < n_sp + 2))
         def _():
-            p = s - 1
+            p = s - 2
             a_y(p).wait_recv()
-            qs[p % 4, y, :, 0] = (qs[p % 4, y, :, 0].astype(F32) + r2y[p].astype(F32)).astype(BF16)
-            t = qs[p % 4, :, x, 1].astype(F32)
+            qs[p % SLOTS, y, :, 0] = (qs[p % SLOTS, y, :, 0].astype(F32) + r2y[p].astype(F32)).astype(BF16)
+            t = qs[p % SLOTS, :, x, 1].astype(F32)
             for j in range(1, X):
                 a_x(p, j).wait_recv()
                 t = t + r2x[p, j - 1].astype(F32)
-            qs[p % 4, :, x, 1] = t.astype(BF16)
+            qs[p % SLOTS, :, x, 1] = t.astype(BF16)
             b_y(p).start()
             for j in range(1, X):
                 b_x(p, j).start()
@@ -539,23 +561,23 @@
         def _():
             to_sib(s).wait_recv()
             own = ret[: 2 * X * mine, :cols].reshape(2, X, 2, hm, cols)
-            qs[s % 4] = (own.astype(BF16).astype(F32) + r1[s].astype(F32)).astype(BF16)
+            qs[s % SLOTS] = (own.astype(BF16).astype(F32) + r1[s].astype(F32)).astype(BF16)
             a_y(s).start()
             for j in range(1, X):
                 a_x(s, j).start()
 
-        @pl.when(s >= 2)
+        @pl.when(s >= 4)
         def _():
-            p = s - 2
+            p = s - 4
             u = block_of(p)
             at = pl.ds(pl.multiple_of(u * cols, cols), cols)
-            t = upd[:hm, at].astype(F32) + qs[p % 4, y, x, 0].astype(F32)
+            t = upd[:hm, at].astype(F32) + qs[p % SLOTS, y, x, 0].astype(F32)
             for j in range(1, X):
                 b_x(p, j).wait_recv()
                 t = t + r3x[p, j - 1].astype(F32)
             out[:hm, at] = t.astype(BF16)
             b_y(p).wait_recv()
-            t = upd[hm:, at].astype(F32) + qs[p % 4, y, x, 1].astype(F32) + r3y[p].astype(F32)
+            t = upd[hm:, at].astype(F32) + qs[p % SLOTS, y, x, 1].astype(F32) + r3y[p].astype(F32)
             out[hm:, at] = t.astype(BF16)
             a_y(p).wait_send()
             b_y(p).wait_send()
@@ -565,7 +587,7 @@
 
         return carry
 
-    lax.fori_loop(0, n_sp + 2, step, 0)
+    lax.fori_loop(0, n_sp + 4, step, 0)
     for s in (n_sp - 2, n_sp - 1):
         to_sib(s).wait_send()
     for cond, end in pending:
@@ -601,11 +623,11 @@
         V((mine, d), F32), V((mine, d), BF16),
         V((2, 2, X, mine, d), BF16), V((n_sp, part, half), BF16), V((n_sp, half, cols), BF16),
         V((2, 2, X, 2, mine // 2, cols), BF16),
-        V((4, 2, X, 2, mine // 2, cols), BF16), V((n_sp, 2, X, 2, mine // 2, cols), BF16),
+        V((SLOTS, 2, X, 2, mine // 2, cols), BF16), V((n_sp, 2, X, 2, mine // 2, cols), BF16),
         V((n_sp, X, mine // 2, cols), BF16), V((n_sp, X - 1, 2, mine // 2, cols), BF16),
         V((n_sp, mine // 2, cols), BF16), V((n_sp, X - 1, mine // 2, cols), BF16),
-        dma((7 + 2 * X * mine // hv,)), dma((2, n_sp, 2)), dma((2, n_sp)), dma((3,)), dma((3,)),
-        dma((4, heads)), dma((4, heads)), dma((X,)), dma((X,)), dma((X, ROWS)), dma((X, ROWS)),
+        dma((7 + 2 * X * mine // hv,)), dma((2, n_sp, 2)), dma((2, n_sp)), dma((2,)), dma((2,)),
+        dma((4, heads)), dma((4, heads)), dma((X, 2)), dma((X, 2)), dma((X, ROWS)), dma((X, ROWS)),
         dma((4, X, ROWS)), dma((X, ROWS)), dma((X, ROWS)), dma((2, X, ROWS)),
         dma((4 + 2 * X, n_sp)), dma((4 + 2 * X, n_sp)),
     ]

time: 187 us -> 165 us (0.88)
  Pallas kernels: 183 us -> 161 us
    pallas_call x1, Pallas kernels: 183 us -> 161 us  [body(): pl.pallas_call(functools.partial(kernel, n_sp, n_tp), in_specs=[anym] * 5...]
where the time goes in v1:
time: 165 us
  Pallas kernels  161 us (98%)
  local copies, waits for them, and re-layouts  3.59 us (2%)
    pallas_call x1, Pallas kernels, body(): pl.pallas_call(functools.partial(kernel, n_sp, n_tp), in_specs=[anym] * 5...  161 us

profile of v1, /device:TPU:24, one launch (start us, length us, event | category | flops | bytes accessed | tf_op | source)
XLA Modules:
  0.0 164.9 jit_solution(5307094709024163544)
XLA Ops:
  0.0 1.3 reshape.3.gain
  1.3 161.3 %layer.1 = bf16[256,2048]{1,0:T(8,128)(2,1)} custom-call(bf16[256,2048]{1,0:T(8,128)(2,1)} %resid_h.1, bf16[1024,512]{1,0:T(8,128)(2,1)} %q_h.1, bf16[1024,512]{1,0:T(8,128)(2,1)} %k_h.1, bf16[1024,1024]{1,0:T(8,128)(2,1)} %v_h.1, bf16[1024,1024]{1,0:T(8,128)(2,1)} %g_h.1, f32[2,1024]{1,0:T(2,128)} %ld.1, bf16[1024,2048]{1,0:T(8,128)(2,1)} %wo_h.1, ...), custom_call_target="tpu_custom_call" | custom-call | tf_op jit(solution)/shard_map/layer/pallas_call | solution.py:634
  162.6 2.3 %copy.16 = bf16[256,2048]{1,0:T(8,128)(2,1)} copy(bf16[256,2048]{1,0:T(8,128)(2,1)} %layer.1) | data formatting | bytes 2097152

commit v2 on v1

--- a/solution.py
+++ b/solution.py
@@ -13,7 +13,7 @@
 BLOCK = 128
 SPAN = 256
 ROWS = 4
-SLOTS = 6
+SLOTS = 5
 EPS = 1e-06
 F32 = jnp.float32
 BF16 = jnp.bfloat16
@@ -37,12 +37,12 @@
 
 def kernel(
     n_sp, n_tp,
-    resid_h, q_h, k_h, v_h, g_h, ld, wo_h, gain, up_h, dn_h, lo_c, lo_s, hi_c, hi_s,
-    out,
-    q_v, k_v, v_v, g_v, wide, res_v, kr, kd, stf, sth, strun, yst, tot, ytot, crecv, csend, esend, inc, ret,
+    resid_h, q_h, k_h, v_h, g_h, ld_h, wo_h, gain, up_h, dn_h, low_h, high_h,
+    out_h,
+    ld, low, high, out, q_v, k_v, v_v, g_v, wide, res_v, kr, kd, stf, sth, strun, yst, tot, ytot, crecv, csend, esend, inc, ret,
     pp, pr, psum, xr, acc, upd, x_all, up_all, dn_all, pd, qs, r1, r2y, r2x, r3y, r3x,
-    lsem, wsend, wrecv, wysend, wyrecv, ssend, srecv, psend, precv, xsend, xrecv,
-    asend, arx, ary, ard, rsend, rrecv,
+    lsem, wsend, wrecv, wlast, wysend, wyrecv, ssend, srecv, psend, precv, xsend, xrecv,
+    asend, arx, ary, ard, dsem, drecv, qsem, qrecv, osem,
 ):
     Z, X = n_sp // 2, n_tp // 2
     sp, tp = lax.axis_index("sp"), lax.axis_index("tp")
@@ -57,6 +57,8 @@
     nblk, nspan = rows // BLOCK, rows // SPAN
     rc = mine // ROWS
     has_up, has_dn = z < Z - 1, z > 0
+    halves = cols % 256 == 0 and Z > 2
+    cw = cols // 2
 
     def rcopy(src, dst, ss, rs, dev):
         return pltpu.make_async_remote_copy(src, dst, ss, rs, device_id=dev, device_id_type=MESH)
@@ -73,18 +75,19 @@
 
     pending = []
 
-    def send(src, dst, ss, rs, dev, cond=None):
+    def send(src, dst, ss, rs, dev, cond=None, track=True):
         def go():
             rcopy(src, dst, ss, rs, dev).start()
-
-        def end():
-            rcopy(src, dst, ss, rs, dev).wait_send()
 
         if cond is None:
             go()
         else:
             pl.when(cond)(go)
-        pending.append((cond, end))
+        if track:
+            sent(src, ss, cond)
+
+    def sent(ref, ss, cond=None):
+        pending.append((cond, lambda: rcopy(ref, ref, ss, ss, to_c).wait_send()))
 
     def recv(dst, ss, rs):
         rcopy(dst, dst, ss, rs, to_c).wait_recv()
@@ -97,12 +100,13 @@
     hv = v_v.shape[1]
     stack = wide.shape[0] // hv
     wc = d // stack
+    loads += [(ld_h, ld), (low_h, low), (high_h, high)]
     loads += [(wo_h.at[:, pl.ds(i * wc, wc)], wide.at[pl.ds(i * hv, hv)]) for i in range(stack)]
 
     def load(i):
         return pltpu.make_async_copy(loads[i][0], loads[i][1], lsem.at[i])
 
-    for i in range(len(loads)):
+    for i in (7, 8, 9, 0, 1):
         load(i).start()
 
     barrier = pltpu.get_barrier_semaphore()
@@ -123,9 +127,12 @@
     o_dn = dn_h.at[pl.ds(pl.multiple_of((1 - y) * half, half), half), :]
     alls = (up_all, dn_all)
 
+    def zsem(w, piece, way):
+        return wsend.at[w, n_sp + piece % 2 if way else piece]
+
     def zsend(w, piece, src, way):
         dev, cond = ((to_zp, has_up), (to_zm, has_dn))[way]
-        send(src, alls[w].at[piece], wsend.at[w, piece, way], wrecv.at[w, piece], dev, cond)
+        send(src, alls[w].at[piece], zsem(w, piece, way), wrecv.at[w, piece], dev, cond)
 
     late = z >= 2
     early = jnp.logical_not(late)
@@ -134,7 +141,7 @@
     zsend(1, sp, h_dn, 1)
 
     def own_dn():
-        return rcopy(h_dn, dn_all.at[sp], wsend.at[1, sp, 0], wrecv.at[1, sp], to_zp)
+        return rcopy(h_dn, dn_all.at[sp], zsem(1, sp, 0), wrecv.at[1, sp], to_zp)
 
     @pl.when(late & has_up)
     def _():
@@ -154,15 +161,18 @@
         parts = []
         low, high = (z - k) * 2 + yy, (z + k) * 2 + yy
         for piece, way, cond in ((low, 0, (z >= k) & has_up), (high, 1, (z + k < Z) & has_dn)):
-            def copy(piece=piece, way=way):
-                ref = alls[w].at[piece]
-                return rcopy(ref, ref, wsend.at[w, piece, way], wrecv.at[w, piece], (to_zp, to_zm)[way])
-
-            def go(copy=copy):
-                copy().wait_recv()
-                copy().start()
-
-            pending.append((cond, lambda copy=copy: copy().wait_send()))
+            ref, sem, dev = alls[w].at[piece], wsend.at[w, piece], (to_zp, to_zm)[way]
+
+            def go(ref=ref, sem=sem, dev=dev, piece=piece):
+                recv(ref, sem, wrecv.at[w, piece])
+                if halves and (w, k, yy) == (1, Z - 2, 1):
+                    for h in range(2):
+                        part = ref.at[:, pl.ds(h * cw, cw)]
+                        rcopy(part, part, sem, wlast.at[h], dev).start()
+                else:
+                    rcopy(ref, ref, sem, wrecv.at[w, piece], dev).start()
+
+            sent(ref, sem, cond)
             parts.append((cond, go))
         return parts
 
@@ -177,12 +187,12 @@
 
         @pl.when(cond)
         def _():
-            recv(alls[w].at[piece], wsend.at[w, piece, 0], wrecv.at[w, piece])
+            recv(alls[w].at[piece], wsend.at[w, piece], wrecv.at[w, piece])
 
     def angles(b):
         at = sp * nblk + b
-        hc, hs = hi_c[pl.ds(at, 1), :], hi_s[pl.ds(at, 1), :]
-        lc, ls = lo_c[...], lo_s[...]
+        hc, hs = high[0, pl.ds(at, 1), :], high[1, pl.ds(at, 1), :]
+        lc, ls = low[0], low[1]
         return hc * lc - hs * ls, hs * lc + hc * ls
 
     def rotated(blk, co, si):
@@ -190,7 +200,10 @@
         return jnp.concatenate([a * co - b * si, a * si + b * co], axis=1)
 
     tot[...] = jnp.zeros_like(tot)
-    load(0).wait()
+    for i in (2, 3, *range(10, len(loads)), 4, 5, 6):
+        load(i).start()
+    for i in (7, 8, 9, 0):
+        load(i).wait()
     for h in range(heads):
         def state_block(t, after, h=h):
             b = nblk - 1 - t
@@ -212,8 +225,9 @@
             part = s[:, p * DV // 2 : (p + 1) * DV // 2]
             stf[p, h] = part
             sth[p, h] = part.astype(BF16)
-        send(sth.at[1 - y, h], yst.at[h], ssend.at[0, h], srecv.at[0, h], to_y)
-    send(tot, ytot, ssend.at[3, 0], srecv.at[3, 0], to_y)
+        send(sth.at[1 - y, h], yst.at[h], ssend.at[0], srecv.at[0], to_y, track=False)
+    sent(sth.at[1 - y], ssend.at[0])
+    send(tot, ytot, ssend.at[3], srecv.at[2], to_y)
     ysend(0, o_up)
     ysend(1, o_dn)
 
@@ -251,7 +265,8 @@
     local(0)
 
     first = y == 0
-    recv(ytot, ssend.at[3, 0], srecv.at[3, 0])
+    recv(ytot, ssend.at[3], srecv.at[2])
+    recv(yst, ssend.at[0], srecv.at[0])
 
     def decays(h):
         own, oth = tot[h : h + 1, : DV // 2], ytot[h : h + 1, : DV // 2]
@@ -260,9 +275,6 @@
     @pl.when(jnp.logical_not(has_dn))
     def _():
         crecv[...] = jnp.zeros_like(crecv)
-
-    def combine(h):
-        recv(yst.at[h], ssend.at[0, h], srecv.at[0, h])
 
     def s_pair(h):
         own, oth = stf[y, h], yst[h].astype(F32)
@@ -274,10 +286,8 @@
         csend[h] = (d0 * d1 * crecv[h].astype(F32) + (d1 * s0 + s1)).astype(BF16)
 
     def chain_send(h):
-        rcopy(csend.at[h], crecv.at[h], ssend.at[1, h], srecv.at[1, h], to_zp).start()
-
-    for h in range(heads):
-        combine(h)
+        rcopy(csend.at[h], crecv.at[h], ssend.at[1], srecv.at[3 + h], to_zp).start()
+
     @pl.when(jnp.logical_not(has_dn))
     def _():
         for h in range(heads):
@@ -290,7 +300,7 @@
 
     def part_up(part):
         ref = up_all.at[other, pl.ds(part * hr, hr)]
-        rcopy(ref, ref, wsend.at[0, other, 0], wrecv.at[0, other], to_zp).start()
+        rcopy(ref, ref, zsem(0, other, 0), wrecv.at[0, other], to_zp).start()
 
     @pl.when(late)
     def _():
@@ -300,7 +310,7 @@
     @pl.when(has_dn)
     def _():
         for h in range(heads):
-            recv(crecv.at[h], ssend.at[1, h], srecv.at[1, h])
+            recv(crecv.at[h], ssend.at[1], srecv.at[3 + h])
 
             @pl.when(has_up)
             def _():
@@ -312,9 +322,8 @@
             own_dn().start()
 
     def chain_end():
-        for h in range(heads):
-            rcopy(csend.at[h], crecv.at[h], ssend.at[1, h], srecv.at[1, h], to_zp).wait_send()
-        rcopy(up_all.at[other], up_all.at[other], wsend.at[0, other, 0], wrecv.at[0, other], to_zp).wait_send()
+        rcopy(csend, crecv, ssend.at[1], srecv.at[0], to_zp).wait_send()
+        rcopy(up_all.at[other], up_all.at[other], zsem(0, other, 0), wrecv.at[0, other], to_zp).wait_send()
 
     pending.append((has_up, chain_end))
     for h in range(heads):
@@ -324,7 +333,7 @@
         later = (d0 * got + s0).astype(BF16)
         inc[y, h] = jnp.where(first, crecv[h], later)
         esend[h] = jnp.where(first, later, crecv[h])
-        send(esend.at[h], inc.at[y, h], ssend.at[2, h], srecv.at[2, h], to_y)
+        send(esend.at[h], inc.at[y, h], ssend.at[2], srecv.at[1], to_y, track=False)
     @pl.when(early)
     def _():
         recv_y(0)
@@ -335,9 +344,9 @@
     fwd(0, 1, y)
     load(3).wait()
     for i in range(stack):
-        load(7 + i).wait()
-    for h in range(heads):
-        recv(inc.at[1 - y, h], ssend.at[2, h], srecv.at[2, h])
+        load(10 + i).wait()
+    sent(esend, ssend.at[2])
+    recv(inc.at[1 - y], ssend.at[2], srecv.at[1])
 
     ph = mine // 2
     fr = min(128, ph)
@@ -378,7 +387,7 @@
             pp[j, mid, at] = val.astype(BF16)
 
         project(base, put)
-        send(pp.at[j, mid], pr.at[j, mid], psend.at[j, p], precv.at[j, p], to_c)
+        send(pp.at[j, mid], pr.at[j, mid], psend.at[j], precv.at[j, p], to_c, track=False)
 
     def for_mine(j, p):
         base = (xat(j) * 2 + c) * mine + p * ph
@@ -389,12 +398,12 @@
             acc[mid, at] = val.astype(BF16).astype(F32)
 
         project(base, put)
-        recv(pr.at[j, mid], psend.at[j, p], precv.at[j, p])
+        recv(pr.at[j, mid], psend.at[j], precv.at[j, p])
         if j:
             for r in range(p * ROWS // 2, (p + 1) * ROWS // 2):
                 at = pl.ds(r * rc, rc)
                 psum[j - 1, at, :] = (acc[at, :] + pr[j, at, :].astype(F32)).astype(BF16)
-                send(psum.at[j - 1, at], xr.at[j - 1, at], xsend.at[j - 1, r], xrecv.at[j - 1, r], to_x(j))
+                send(psum.at[j - 1, at], xr.at[j - 1, at], xsend.at[j - 1], xrecv.at[j - 1, r], to_x(j), track=False)
 
     for j in range(1, X):
         for p in range(2):
@@ -409,23 +418,28 @@
         zsend(1, other, dn_all.at[other], way)
     fwd(0, 2, y)
 
+    for j in range(X):
+        sent(pp.at[j], psend.at[j])
+        if j:
+            sent(psum.at[j - 1], xsend.at[j - 1])
+
     load(4).wait()
     for r in range(ROWS):
         at = pl.ds(r * rc, rc)
         s = acc[at, :] + pr[0, at, :].astype(F32)
         for j in range(1, X):
-            recv(xr.at[j - 1, at], xsend.at[j - 1, r], xrecv.at[j - 1, r])
+            recv(xr.at[j - 1, at], xsend.at[j - 1], xrecv.at[j - 1, r])
             s = s + xr[j - 1, at, :].astype(F32)
         u = (res_v[at, :].astype(F32) + s).astype(BF16)
         upd[at, :] = u
         u = u.astype(F32)
         u = u * lax.rsqrt(jnp.mean(u * u, axis=1, keepdims=True) + EPS)
-        x_all[c, y, x, at, :] = (u * gain[...].astype(F32)).astype(BF16)
+        x_all[c, y, x, at, :] = (u * gain[...].astype(F32).reshape(1, d)).astype(BF16)
         own = x_all.at[c, y, x, at]
-        send(own, own, asend.at[0, 0, r], ary.at[0, r], to_y)
+        send(own, own, asend.at[0, 0], ary.at[0, r], to_y, track=False)
         for j in range(1, X):
-            send(own, own, asend.at[1, j, r], arx.at[j, r], to_x(j))
-        send(own, own, asend.at[2, 0, r], ard.at[0, 0, r], to_c)
+            send(own, own, asend.at[1, j], arx.at[j, r], to_x(j), track=False)
+        send(own, own, asend.at[2, 0], ard.at[0, 0], to_c, track=False)
 
     load(5).wait()
     for k in range(1, Z - 1):
@@ -455,20 +469,24 @@
 
         lax.fori_loop(0, half // ht, part, 0)
 
-    def from_sibling(yrel, i, r):
-        at = pl.ds(r * rc, rc)
-        dst = x_all.at[1 - c, jnp.where(yrel == 0, y, 1 - y), xat(-i), at]
-        recv(dst, asend.at[2, 0, r], ard.at[yrel, i, r])
+    for i in range(X):
+        for kind, yy in ((0, y), (2, y), (3, 1 - y)):
+            sent(x_all.at[c, yy, xat(-i)], asend.at[kind, i])
+        if i:
+            sent(x_all.at[c, y, x], asend.at[1, i])
+
+    def from_sibling(yrel, i):
+        recv(x_all.at[1 - c, (1 - y) if yrel else y, xat(-i)], asend.at[2, 0], ard.at[yrel, i])
 
     def pass_on(yrel, i, r):
         at = pl.ds(r * rc, rc)
         ref = x_all.at[c, (1 - y) if yrel else y, xat(-i), at]
         if yrel:
-            recv(ref, asend.at[0, 0, r], ary.at[i, r])
+            recv(ref, asend.at[0, 0], ary.at[i, r])
         else:
-            recv(ref, asend.at[1, i, r], arx.at[i, r])
-            send(ref, ref, asend.at[0, i, r], ary.at[i, r], to_y)
-        send(ref, ref, asend.at[2 + yrel, i, r], ard.at[yrel, i, r], to_c)
+            recv(ref, asend.at[1, i], arx.at[i, r])
+            send(ref, ref, asend.at[0, i], ary.at[i, r], to_y, track=False)
+        send(ref, ref, asend.at[2 + yrel, i], ard.at[yrel, i], to_c, track=False)
 
     for r in range(ROWS):
         pass_on(1, 0, r)
@@ -480,21 +498,17 @@
     fwd(1, 1, 1)
     for k in range(n_sp):
         settle(0, k)
-    for r in range(ROWS):
-        from_sibling(0, 0, r)
+    from_sibling(0, 0)
     hidden(y, x)
-    for r in range(ROWS):
-        from_sibling(1, 0, r)
+    from_sibling(1, 0)
     hidden(1 - y, x)
     for j in range(1, X):
         for r in range(ROWS):
             pass_on(1, j, r)
-        for r in range(ROWS):
-            from_sibling(0, j, r)
+        from_sibling(0, j)
         hidden(y, xat(-j))
     for j in range(1, X):
-        for r in range(ROWS):
-            from_sibling(1, j, r)
+        from_sibling(1, j)
         hidden(1 - y, xat(-j))
 
     load(6).wait()
@@ -507,20 +521,93 @@
         far = jnp.where(z <= Z - 1 - z, i, Z - 1 - i)
         return jnp.where(i <= 2 * m, near, far) * 2 + s % 2
 
-    def to_sib(s):
-        return rcopy(pd.at[s % 2], r1.at[s], rsend.at[0, s], rrecv.at[0, s], to_c)
-
-    def a_y(s):
-        return rcopy(qs.at[s % SLOTS, 1 - y, :, 0], r2y.at[s], rsend.at[1, s], rrecv.at[1, s], to_y)
-
-    def a_x(s, j):
-        return rcopy(qs.at[s % SLOTS, :, xat(j), 1], r2x.at[s, j - 1], rsend.at[3 + j, s], rrecv.at[3 + j, s], to_x(j))
-
-    def b_y(s):
-        return rcopy(qs.at[s % SLOTS, 1 - y, x, 1], r3y.at[s], rsend.at[2, s], rrecv.at[2, s], to_y)
-
-    def b_x(s, j):
-        return rcopy(qs.at[s % SLOTS, y, xat(j), 0], r3x.at[s, j - 1], rsend.at[3 + X + j, s], rrecv.at[3 + X + j, s], to_x(j))
+    units = n_sp - 1 if halves else n_sp
+    total = units + 2 if halves else units
+    na, nb = 3 * X - 2, X
+
+    class Unit:
+        def __init__(self, t, part=None):
+            self.t, self.u = t, (t if part is None else n_sp - 1)
+            self.w = cols if part is None else cw
+            self.c0 = 0 if part is None else part * cw
+            self.block = block_of(self.u)
+
+        def trim(self, ref, start):
+            return ref if self.w == cols else ref.at[..., pl.ds(start, self.w)]
+
+        def bulk(self, n, ss, rs):
+            ref = wide.at[pl.ds(0, n * hm), pl.ds(0, self.w)]
+            return rcopy(ref, ref, ss, rs, to_c)
+
+        def to_sib(self):
+            t = self.t
+            return rcopy(self.trim(pd.at[t % 2], 0), self.trim(r1.at[self.u], self.c0), dsem.at[t % 2], drecv.at[t], to_c)
+
+        def copies(self, stage):
+            q, t, u = qs.at[self.t % SLOTS], self.t, self.u
+            if stage == 0:
+                pairs = [(q.at[1 - y, :, 0], r2y.at[u], to_y)]
+                pairs += [(q.at[:, xat(j), 1], r2x.at[u, j - 1], to_x(j)) for j in range(1, X)]
+            else:
+                pairs = [(q.at[1 - y, x, 1], r3y.at[u], to_y)]
+                pairs += [(q.at[y, xat(j), 0], r3x.at[u, j - 1], to_x(j)) for j in range(1, X)]
+            for src, dst, dev in pairs:
+                rcopy(self.trim(src, 0), self.trim(dst, self.c0), qsem.at[stage, t % SLOTS], qrecv.at[stage, t], dev).start()
+
+        def wait_sib(self):
+            ref = self.trim(pd.at[self.t % 2], 0)
+            rcopy(ref, ref, dsem.at[self.t % 2], drecv.at[self.t], to_c).wait_send()
+
+        def compute(self, before):
+            if self.w == cols:
+                settle(1, self.block)
+            else:
+                @pl.when(jnp.logical_not(has_up & has_dn))
+                def _():
+                    ref = dn_all.at[self.block, :, pl.ds(self.c0, cw)]
+                    recv(ref, wsend.at[1, 0], wlast.at[self.c0 // cw])
+            if before is not None:
+                before()
+            w = dn_all[self.block, :, self.c0 : self.c0 + self.w]
+            pd[self.t % 2, :, :, :, :, : self.w] = dot(wide[:, hid_of(1 - c)], w).astype(BF16).reshape(2, X, 2, hm, self.w)
+            self.to_sib().start()
+            ret[: 2 * X * mine, : self.w] = dot(wide[:, hid_of(c)], w)
+
+        def first(self):
+            k, at = self.t % SLOTS, slice(self.c0, self.c0 + self.w)
+            self.to_sib().wait_recv()
+            own = ret[: 2 * X * mine, : self.w].reshape(2, X, 2, hm, self.w)
+            qs[k, :, :, :, :, : self.w] = (own.astype(BF16).astype(F32) + r1[self.u, :, :, :, :, at].astype(F32)).astype(BF16)
+            self.copies(0)
+
+        def second(self):
+            k, at, w = self.t % SLOTS, slice(self.c0, self.c0 + self.w), self.w
+            self.bulk(na, qsem.at[0, 0], qrecv.at[0, self.t]).wait_recv()
+            qs[k, y, :, 0, :, :w] = (qs[k, y, :, 0, :, :w].astype(F32) + r2y[self.u, :, :, at].astype(F32)).astype(BF16)
+            s = qs[k, :, x, 1, :, :w].astype(F32)
+            for j in range(1, X):
+                s = s + r2x[self.u, j - 1, :, :, at].astype(F32)
+            qs[k, :, x, 1, :, :w] = s.astype(BF16)
+            self.copies(1)
+
+        def put(self):
+            at = pl.ds(pl.multiple_of(self.block * cols + self.c0, 128), self.w)
+            return pltpu.make_async_copy(self.trim(out.at[self.t % 4], 0), out_h.at[:, at], osem.at[self.t % 4])
+
+        def final(self):
+            k, at, w = self.t % SLOTS, slice(self.c0, self.c0 + self.w), self.w
+            o = self.t % 4
+            col = pl.ds(pl.multiple_of(self.block * cols + self.c0, 128), w)
+            self.bulk(nb, qsem.at[1, 0], qrecv.at[1, self.t]).wait_recv()
+            s = upd[:hm, col].astype(F32) + qs[k, y, x, 0, :, :w].astype(F32)
+            for j in range(1, X):
+                s = s + r3x[self.u, j - 1, :, at].astype(F32)
+            out[o, :hm, :w] = s.astype(BF16)
+            s = upd[hm:, col].astype(F32) + qs[k, y, x, 1, :, :w].astype(F32) + r3y[self.u, :, at].astype(F32)
+            out[o, hm:, :w] = s.astype(BF16)
+            self.put().start()
+            self.bulk(na, qsem.at[0, k], qrecv.at[0, 0]).wait_send()
+            self.bulk(nb, qsem.at[1, k], qrecv.at[1, 0]).wait_send()
 
     last = [(2 * (k - 2 + yy), relays(1, k, yy)) for k in range(2, Z - 1) for yy in range(2)]
 
@@ -528,68 +615,42 @@
         for at, parts in last:
             for cond, go in parts:
                 pl.when(cond & (s == at))(go)
-
-        @pl.when(s < n_sp)
+        Unit(s).compute(lambda: pl.when(s >= 2)(lambda: Unit(s - 2).wait_sib()))
+
+        @pl.when(s >= 2)
         def _():
-            u = block_of(s)
-            settle(1, u)
-
-            @pl.when(s >= 2)
-            def _():
-                to_sib(s - 2).wait_send()
-
-            w = dn_all[u]
-            pd[s % 2] = dot(wide[:, hid_of(1 - c)], w).astype(BF16).reshape(2, X, 2, hm, cols)
-            to_sib(s).start()
-            ret[: 2 * X * mine, :cols] = dot(wide[:, hid_of(c)], w)
-
-        @pl.when((s >= 2) & (s < n_sp + 2))
-        def _():
-            p = s - 2
-            a_y(p).wait_recv()
-            qs[p % SLOTS, y, :, 0] = (qs[p % SLOTS, y, :, 0].astype(F32) + r2y[p].astype(F32)).astype(BF16)
-            t = qs[p % SLOTS, :, x, 1].astype(F32)
-            for j in range(1, X):
-                a_x(p, j).wait_recv()
-                t = t + r2x[p, j - 1].astype(F32)
-            qs[p % SLOTS, :, x, 1] = t.astype(BF16)
-            b_y(p).start()
-            for j in range(1, X):
-                b_x(p, j).start()
-
-        @pl.when(s < n_sp)
-        def _():
-            to_sib(s).wait_recv()
-            own = ret[: 2 * X * mine, :cols].reshape(2, X, 2, hm, cols)
-            qs[s % SLOTS] = (own.astype(BF16).astype(F32) + r1[s].astype(F32)).astype(BF16)
-            a_y(s).start()
-            for j in range(1, X):
-                a_x(s, j).start()
+            Unit(s - 2).second()
+
+        Unit(s).first()
 
         @pl.when(s >= 4)
         def _():
-            p = s - 4
-            u = block_of(p)
-            at = pl.ds(pl.multiple_of(u * cols, cols), cols)
-            t = upd[:hm, at].astype(F32) + qs[p % SLOTS, y, x, 0].astype(F32)
-            for j in range(1, X):
-                b_x(p, j).wait_recv()
-                t = t + r3x[p, j - 1].astype(F32)
-            out[:hm, at] = t.astype(BF16)
-            b_y(p).wait_recv()
-            t = upd[hm:, at].astype(F32) + qs[p % SLOTS, y, x, 1].astype(F32) + r3y[p].astype(F32)
-            out[hm:, at] = t.astype(BF16)
-            a_y(p).wait_send()
-            b_y(p).wait_send()
-            for j in range(1, X):
-                a_x(p, j).wait_send()
-                b_x(p, j).wait_send()
+            pl.when(s >= 8)(lambda: Unit(s - 8).put().wait())
+            Unit(s - 4).final()
 
         return carry
 
-    lax.fori_loop(0, n_sp + 4, step, 0)
-    for s in (n_sp - 2, n_sp - 1):
-        to_sib(s).wait_send()
+    lax.fori_loop(0, units, step, 0)
+    tail = [Unit(t) for t in range(units)]
+    if halves:
+        tail += [Unit(units + p, p) for p in range(2)]
+        for t in range(units, total):
+            tail[t].compute(tail[t - 2].wait_sib)
+            tail[t - 2].second()
+            tail[t].first()
+            if t >= 8:
+                tail[t - 8].put().wait()
+            tail[t - 4].final()
+    tail[total - 2].second()
+    tail[total - 1].second()
+    for t in range(total - 4, total):
+        if t >= 4:
+            tail[t - 4].put().wait()
+        tail[t].final()
+    for t in range(total - 4, total):
+        tail[t].put().wait()
+    for t in range(total - 2, total):
+        tail[t].wait_sib()
     for cond, end in pending:
         if cond is None:
             end()
@@ -603,15 +664,16 @@
     mine, d = resid.shape
     half, cols, part = up.shape[1] // 2, down.shape[1], up.shape[0]
     freq = 10000.0 ** (-np.arange(0, DK, 2, dtype=np.float64) / DK)
-    low = np.arange(BLOCK)[:, None] * freq[None, :]
-    high = (BLOCK * np.arange(rows * n_sp // BLOCK))[:, None] * freq[None, :]
-    tables = [jnp.asarray(f(a), F32) for a in (low, high) for f in (np.cos, np.sin)]
+    near = np.arange(BLOCK)[:, None] * freq[None, :]
+    far = (BLOCK * np.arange(rows * n_sp // BLOCK))[:, None] * freq[None, :]
+    tables = [jnp.asarray(np.stack([np.cos(a), np.sin(a)]), F32) for a in (near, far)]
     vm, anym = pl.BlockSpec(memory_space=pltpu.VMEM), pl.BlockSpec(memory_space=pl.ANY)
     dma = pltpu.SemaphoreType.DMA
     V = pltpu.VMEM
     hd, hv = heads * DK, heads * DV
     sq = (DK, DV // 2)
     scratch = [
+        V((heads, rows), F32), *[V(t.shape, F32) for t in tables], V((4, mine, cols), BF16),
         V((rows, hd), BF16), V((rows, hd), BF16), V((rows, hv), BF16), V((rows, hv), BF16),
         V((2 * X * mine, 2 * half), BF16), V((mine, d), BF16),
         V((heads, rows, DK), BF16), V((rows, DK), BF16),
@@ -626,22 +688,22 @@
         V((SLOTS, 2, X, 2, mine // 2, cols), BF16), V((n_sp, 2, X, 2, mine // 2, cols), BF16),
         V((n_sp, X, mine // 2, cols), BF16), V((n_sp, X - 1, 2, mine // 2, cols), BF16),
         V((n_sp, mine // 2, cols), BF16), V((n_sp, X - 1, mine // 2, cols), BF16),
-        dma((7 + 2 * X * mine // hv,)), dma((2, n_sp, 2)), dma((2, n_sp)), dma((2,)), dma((2,)),
-        dma((4, heads)), dma((4, heads)), dma((X, 2)), dma((X, 2)), dma((X, ROWS)), dma((X, ROWS)),
-        dma((4, X, ROWS)), dma((X, ROWS)), dma((X, ROWS)), dma((2, X, ROWS)),
-        dma((4 + 2 * X, n_sp)), dma((4 + 2 * X, n_sp)),
+        dma((10 + 2 * X * mine // hv,)), dma((2, n_sp + 2)), dma((2, n_sp)), dma((2,)), dma((2,)), dma((2,)),
+        dma((4,)), dma((3 + heads,)), dma((X,)), dma((X, 2)), dma((X - 1,)), dma((X - 1, ROWS)),
+        dma((4, X)), dma((X, ROWS)), dma((X, ROWS)), dma((2, X)),
+        dma((2,)), dma((n_sp + 1,)), dma((2, SLOTS)), dma((2, n_sp + 1)), dma((4,)),
     ]
     return pl.pallas_call(
         functools.partial(kernel, n_sp, n_tp),
-        in_specs=[anym] * 5 + [vm, anym, vm, anym, anym] + [vm] * 4,
-        out_specs=vm,
+        in_specs=[anym] * 7 + [vm] + [anym] * 4,
+        out_specs=anym,
         out_shape=jax.ShapeDtypeStruct((mine, d), BF16),
         scratch_shapes=scratch,
         compiler_params=pltpu.CompilerParams(
             collective_id=0, has_side_effects=True, vmem_limit_bytes=67043328
         ),
         name="layer",
-    )(resid, queries, keys, values, gates, log_decay, w_out, gain.reshape(1, d), up, down, *tables)
+    )(resid, queries, keys, values, gates, log_decay, w_out, gain, up, down, *tables)
 
 
 def solution(mesh):

time: 165 us -> 159 us (0.964)
  Pallas kernels: 161 us -> 157 us
    pallas_call x1, Pallas kernels: 161 us -> 157 us  [body(): pl.pallas_call(functools.partial(kernel, n_sp, n_tp), in_specs=[anym] * 7...]
where the time goes in v2:
time: 159 us
  Pallas kernels  157 us (99%)
  local copies, waits for them, and re-layouts  2.3 us (1%)
    pallas_call x1, Pallas kernels, body(): pl.pallas_call(functools.partial(kernel, n_sp, n_tp), in_specs=[anym] * 7...  157 us

profile of v2, /device:TPU:24, one launch (start us, length us, event | category | flops | bytes accessed | tf_op | source)
XLA Modules:
  0.0 159.2 jit_solution(3209902914828206687)
XLA Ops:
  0.0 156.9 %layer.1 = bf16[256,2048]{1,0:T(8,128)(2,1)} custom-call(bf16[256,2048]{1,0:T(8,128)(2,1)} %resid_h.1, bf16[1024,512]{1,0:T(8,128)(2,1)} %q_h.1, bf16[1024,512]{1,0:T(8,128)(2,1)} %k_h.1, bf16[1024,1024]{1,0:T(8,128)(2,1)} %v_h.1, bf16[1024,1024]{1,0:T(8,128)(2,1)} %g_h.1, f32[2,1024]{1,0:T(2,128)} %ld_h.1, bf16[1024,2048]{1,0:T(8,128)(2,1)} %wo_h.1, ...), custom_call_target="tpu_custom_call" | custom-call | tf_op jit(solution)/shard_map/layer/pallas_call | solution.py:696
  156.9 2.3 %copy.14 = bf16[256,2048]{1,0:T(8,128)(2,1)} copy(bf16[256,2048]{1,0:T(8,128)(2,1)} %layer.1) | data formatting | bytes 2097152

commit v3 on v2

--- a/solution.py
+++ b/solution.py
@@ -40,7 +40,7 @@
     resid_h, q_h, k_h, v_h, g_h, ld_h, wo_h, gain, up_h, dn_h, low_h, high_h,
     out_h,
     ld, low, high, out, q_v, k_v, v_v, g_v, wide, res_v, kr, kd, stf, sth, strun, yst, tot, ytot, crecv, csend, esend, inc, ret,
-    pp, pr, psum, xr, acc, upd, x_all, up_all, dn_all, pd, qs, r1, r2y, r2x, r3y, r3x,
+    pp, pr, psum, xr, acc, upd, x_all, up_all, dn_all, pd, qs, r1, r2y, r2x, r3y, r3x, rd,
     lsem, wsend, wrecv, wlast, wysend, wyrecv, ssend, srecv, psend, precv, xsend, xrecv,
     asend, arx, ary, ard, dsem, drecv, qsem, qrecv, osem,
 ):
@@ -58,7 +58,8 @@
     rc = mine // ROWS
     has_up, has_dn = z < Z - 1, z > 0
     halves = cols % 256 == 0 and Z > 2
-    cw = cols // 2
+    cw, ka = cols // 2, half - min(256, half // 2)
+    pieces = ((0, half, 0), (0, ka, cw), (ka, half - ka, cw))
 
     def rcopy(src, dst, ss, rs, dev):
         return pltpu.make_async_remote_copy(src, dst, ss, rs, device_id=dev, device_id_type=MESH)
@@ -72,6 +73,9 @@
 
     def to_x(j):
         return {"tp": xat(j) * 2 + c}
+
+    def to_diag(j):
+        return {"sp": z * 2 + (1 - y), "tp": xat(j) * 2 + c}
 
     pending = []
 
@@ -111,6 +115,8 @@
 
     barrier = pltpu.get_barrier_semaphore()
     greet = [(to_y, None), (to_c, None)] + [(to_x(j), None) for j in range(1, X)]
+    if halves:
+        greet += [(to_diag(j), None) for j in range(1, X)]
     greet += [(to_zp, has_up), (to_zm, has_dn)]
     for dev, cond in greet:
         def hello(dev=dev):
@@ -119,7 +125,7 @@
             hello()
         else:
             pl.when(cond)(hello)
-    pl.semaphore_wait(barrier, X + 1 + jnp.where(has_up, 1, 0) + jnp.where(has_dn, 1, 0))
+    pl.semaphore_wait(barrier, X + 1 + halves * (X - 1) + jnp.where(has_up, 1, 0) + jnp.where(has_dn, 1, 0))
 
     h_up = up_h.at[:, pl.ds(pl.multiple_of(y * half, half), half)]
     h_dn = dn_h.at[pl.ds(pl.multiple_of(y * half, half), half), :]
@@ -166,8 +172,8 @@
             def go(ref=ref, sem=sem, dev=dev, piece=piece):
                 recv(ref, sem, wrecv.at[w, piece])
                 if halves and (w, k, yy) == (1, Z - 2, 1):
-                    for h in range(2):
-                        part = ref.at[:, pl.ds(h * cw, cw)]
+                    for h, (r0, nr, c0) in enumerate(pieces):
+                        part = ref.at[pl.ds(r0, nr), pl.ds(c0, cw)]
                         rcopy(part, part, sem, wlast.at[h], dev).start()
                 else:
                     rcopy(ref, ref, sem, wrecv.at[w, piece], dev).start()
@@ -527,7 +533,7 @@
 
     class Unit:
         def __init__(self, t, part=None):
-            self.t, self.u = t, (t if part is None else n_sp - 1)
+            self.t, self.u, self.part = t, (t if part is None else n_sp - 1), part
             self.w = cols if part is None else cw
             self.c0 = 0 if part is None else part * cw
             self.block = block_of(self.u)
@@ -551,27 +557,52 @@
             else:
                 pairs = [(q.at[1 - y, x, 1], r3y.at[u], to_y)]
                 pairs += [(q.at[y, xat(j), 0], r3x.at[u, j - 1], to_x(j)) for j in range(1, X)]
+            if self.part is not None:
+                to = [(1, 0, to_y)] + [(0, j, to_x(j)) for j in range(1, X)] + [(1, j, to_diag(j)) for j in range(1, X)]
+                pairs = [(q.at[(1 - y) if f else y, xat(j)], rd.at[self.part, f * X + j], dev) for f, j, dev in to]
             for src, dst, dev in pairs:
-                rcopy(self.trim(src, 0), self.trim(dst, self.c0), qsem.at[stage, t % SLOTS], qrecv.at[stage, t], dev).start()
+                dst = dst if self.part is not None else self.trim(dst, self.c0)
+                rcopy(self.trim(src, 0), dst, qsem.at[stage, t % SLOTS], qrecv.at[stage, t], dev).start()
 
         def wait_sib(self):
             ref = self.trim(pd.at[self.t % 2], 0)
             rcopy(ref, ref, dsem.at[self.t % 2], drecv.at[self.t], to_c).wait_send()
 
+        def arrive(self, i):
+            r0, nr, c0 = pieces[i]
+
+            @pl.when(jnp.logical_not(has_up & has_dn))
+            def _():
+                ref = dn_all.at[self.block, pl.ds(r0, nr), pl.ds(c0, cw)]
+                recv(ref, wsend.at[1, 0], wlast.at[i])
+
+        def product(self, cls, r0, nr):
+            w = dn_all[self.block, r0 : r0 + nr, self.c0 : self.c0 + self.w]
+            return dot(wide[:, pl.ds(pl.multiple_of(cls * half + r0, 128), nr)], w)
+
         def compute(self, before):
-            if self.w == cols:
+            if self.part is None:
                 settle(1, self.block)
             else:
-                @pl.when(jnp.logical_not(has_up & has_dn))
-                def _():
-                    ref = dn_all.at[self.block, :, pl.ds(self.c0, cw)]
-                    recv(ref, wsend.at[1, 0], wlast.at[self.c0 // cw])
-            if before is not None:
-                before()
-            w = dn_all[self.block, :, self.c0 : self.c0 + self.w]
-            pd[self.t % 2, :, :, :, :, : self.w] = dot(wide[:, hid_of(1 - c)], w).astype(BF16).reshape(2, X, 2, hm, self.w)
+                self.arrive(0)
+            before()
+            self.offer(self.product(1 - c, 0, half))
+            ret[: 2 * X * mine, : self.w] = self.product(c, 0, half)
+
+        def offer(self, value):
+            pd[self.t % 2, :, :, :, :, : self.w] = value.astype(BF16).reshape(2, X, 2, hm, self.w)
             self.to_sib().start()
-            ret[: 2 * X * mine, : self.w] = dot(wide[:, hid_of(c)], w)
+
+        def early(self):
+            self.arrive(1)
+            ret[: 2 * X * mine, cw : 2 * cw] = self.product(1 - c, 0, ka)
+            ret[: 2 * X * mine, 2 * cw : 3 * cw] = self.product(c, 0, ka)
+
+        def late(self, before):
+            self.arrive(2)
+            before()
+            self.offer(ret[: 2 * X * mine, cw : 2 * cw] + self.product(1 - c, ka, half - ka))
+            ret[: 2 * X * mine, :cw] = ret[: 2 * X * mine, 2 * cw : 3 * cw] + self.product(c, ka, half - ka)
 
         def first(self):
             k, at = self.t % SLOTS, slice(self.c0, self.c0 + self.w)
@@ -598,6 +629,16 @@
             k, at, w = self.t % SLOTS, slice(self.c0, self.c0 + self.w), self.w
             o = self.t % 4
             col = pl.ds(pl.multiple_of(self.block * cols + self.c0, 128), w)
+            if self.part is not None:
+                every = (2 * X - 1) * 2
+                self.bulk(every, qsem.at[0, 0], qrecv.at[0, self.t]).wait_recv()
+                s = qs[k, y, x, :, :, :w].astype(F32)
+                for i in range(1, 2 * X):
+                    s = s + rd[self.part, i].astype(F32)
+                out[o, :, :w] = (upd[:, col].astype(F32) + s.reshape(mine, w)).astype(BF16)
+                self.put().start()
+                self.bulk(every, qsem.at[0, k], qrecv.at[0, 0]).wait_send()
+                return
             self.bulk(nb, qsem.at[1, 0], qrecv.at[1, self.t]).wait_recv()
             s = upd[:hm, col].astype(F32) + qs[k, y, x, 0, :, :w].astype(F32)
             for j in range(1, X):
@@ -632,21 +673,29 @@
 
     lax.fori_loop(0, units, step, 0)
     tail = [Unit(t) for t in range(units)]
-    if halves:
-        tail += [Unit(units + p, p) for p in range(2)]
-        for t in range(units, total):
-            tail[t].compute(tail[t - 2].wait_sib)
-            tail[t - 2].second()
-            tail[t].first()
-            if t >= 8:
-                tail[t - 8].put().wait()
-            tail[t - 4].final()
-    tail[total - 2].second()
-    tail[total - 1].second()
-    for t in range(total - 4, total):
+
+    def finish_unit(t):
         if t >= 4:
             tail[t - 4].put().wait()
         tail[t].final()
+
+    if halves:
+        tail += [Unit(units + p, p) for p in range(2)]
+        one, two = tail[units], tail[units + 1]
+        one.compute(tail[units - 2].wait_sib)
+        tail[units - 2].second()
+        two.early()
+        one.first()
+        finish_unit(units - 4)
+        two.late(tail[units - 1].wait_sib)
+        tail[units - 1].second()
+        two.first()
+        finish_unit(units - 3)
+    else:
+        tail[units - 2].second()
+        tail[units - 1].second()
+    for t in range(total - 4, total):
+        finish_unit(t)
     for t in range(total - 4, total):
         tail[t].put().wait()
     for t in range(total - 2, total):
@@ -688,7 +737,8 @@
         V((SLOTS, 2, X, 2, mine // 2, cols), BF16), V((n_sp, 2, X, 2, mine // 2, cols), BF16),
         V((n_sp, X, mine // 2, cols), BF16), V((n_sp, X - 1, 2, mine // 2, cols), BF16),
         V((n_sp, mine // 2, cols), BF16), V((n_sp, X - 1, mine // 2, cols), BF16),
-        dma((10 + 2 * X * mine // hv,)), dma((2, n_sp + 2)), dma((2, n_sp)), dma((2,)), dma((2,)), dma((2,)),
+        V((2, 2 * X, 2, mine // 2, cols // 2), BF16),
+        dma((10 + 2 * X * mine // hv,)), dma((2, n_sp + 2)), dma((2, n_sp)), dma((3,)), dma((2,)), dma((2,)),
         dma((4,)), dma((3 + heads,)), dma((X,)), dma((X, 2)), dma((X - 1,)), dma((X - 1, ROWS)),
         dma((4, X)), dma((X, ROWS)), dma((X, ROWS)), dma((2, X)),
         dma((2,)), dma((n_sp + 1,)), dma((2, SLOTS)), dma((2, n_sp + 1)), dma((4,)),

time: 159 us -> 158 us (level)
  Pallas kernels: 157 us -> 155 us
where the time goes in v3:
time: 158 us
  Pallas kernels  155 us (98%)
  local copies, waits for them, and re-layouts  2.3 us (1%)
    pallas_call x1, Pallas kernels, body(): pl.pallas_call(functools.partial(kernel, n_sp, n_tp), in_specs=[anym] * 7...  155 us

profile of v3, /device:TPU:24, one launch (start us, length us, event | category | flops | bytes accessed | tf_op | source)
XLA Modules:
  0.0 157.8 jit_solution(12204493441860709146)
XLA Ops:
  0.0 155.5 %layer.1 = bf16[256,2048]{1,0:T(8,128)(2,1)} custom-call(bf16[256,2048]{1,0:T(8,128)(2,1)} %resid_h.1, bf16[1024,512]{1,0:T(8,128)(2,1)} %q_h.1, bf16[1024,512]{1,0:T(8,128)(2,1)} %k_h.1, bf16[1024,1024]{1,0:T(8,128)(2,1)} %v_h.1, bf16[1024,1024]{1,0:T(8,128)(2,1)} %g_h.1, f32[2,1024]{1,0:T(2,128)} %ld_h.1, bf16[1024,2048]{1,0:T(8,128)(2,1)} %wo_h.1, ...), custom_call_target="tpu_custom_call" | custom-call | tf_op jit(solution)/shard_map/layer/pallas_call | solution.py:746
  155.5 2.3 %copy.14 = bf16[256,2048]{1,0:T(8,128)(2,1)} copy(bf16[256,2048]{1,0:T(8,128)(2,1)} %layer.1) | data formatting | bytes 2097152

commit v4 on v3

--- a/solution.py
+++ b/solution.py
@@ -38,11 +38,11 @@
 def kernel(
     n_sp, n_tp,
     resid_h, q_h, k_h, v_h, g_h, ld_h, wo_h, gain, up_h, dn_h, low_h, high_h,
-    out_h,
-    ld, low, high, out, q_v, k_v, v_v, g_v, wide, res_v, kr, kd, stf, sth, strun, yst, tot, ytot, crecv, csend, esend, inc, ret,
+    out,
+    ld, low, high, q_v, k_v, v_v, g_v, wide, res_v, kr, kd, stf, sth, strun, yst, tot, ytot, crecv, csend, esend, inc, ret,
     pp, pr, psum, xr, acc, upd, x_all, up_all, dn_all, pd, qs, r1, r2y, r2x, r3y, r3x, rd,
     lsem, wsend, wrecv, wlast, wysend, wyrecv, ssend, srecv, psend, precv, xsend, xrecv,
-    asend, arx, ary, ard, dsem, drecv, qsem, qrecv, osem,
+    asend, arx, ary, ard, dsem, drecv, qsem, qrecv,
 ):
     Z, X = n_sp // 2, n_tp // 2
     sp, tp = lax.axis_index("sp"), lax.axis_index("tp")
@@ -133,12 +133,9 @@
     o_dn = dn_h.at[pl.ds(pl.multiple_of((1 - y) * half, half), half), :]
     alls = (up_all, dn_all)
 
-    def zsem(w, piece, way):
-        return wsend.at[w, n_sp + piece % 2 if way else piece]
-
     def zsend(w, piece, src, way):
         dev, cond = ((to_zp, has_up), (to_zm, has_dn))[way]
-        send(src, alls[w].at[piece], zsem(w, piece, way), wrecv.at[w, piece], dev, cond)
+        send(src, alls[w].at[piece], wsend.at[way, 0], wrecv.at[w, piece], dev, cond, track=False)
 
     late = z >= 2
     early = jnp.logical_not(late)
@@ -147,13 +144,14 @@
     zsend(1, sp, h_dn, 1)
 
     def own_dn():
-        return rcopy(h_dn, dn_all.at[sp], zsem(1, sp, 0), wrecv.at[1, sp], to_zp)
+        return rcopy(h_dn, dn_all.at[sp], wsend.at[0, 0], wrecv.at[1, sp], to_zp)
 
     @pl.when(late & has_up)
     def _():
         own_dn().start()
 
-    pending.append((has_up, lambda: own_dn().wait_send()))
+    for way, cond in enumerate((has_up, has_dn)):
+        sent(up_all.at[pl.ds(0, 4)], wsend.at[way, 0], cond)
     hr = up_h.shape[0] // 2
     other = z * 2 + (1 - y)
 
@@ -167,7 +165,7 @@
         parts = []
         low, high = (z - k) * 2 + yy, (z + k) * 2 + yy
         for piece, way, cond in ((low, 0, (z >= k) & has_up), (high, 1, (z + k < Z) & has_dn)):
-            ref, sem, dev = alls[w].at[piece], wsend.at[w, piece], (to_zp, to_zm)[way]
+            ref, sem, dev = alls[w].at[piece], wsend.at[way, k], (to_zp, to_zm)[way]
 
             def go(ref=ref, sem=sem, dev=dev, piece=piece):
                 recv(ref, sem, wrecv.at[w, piece])
@@ -178,7 +176,8 @@
                 else:
                     rcopy(ref, ref, sem, wrecv.at[w, piece], dev).start()
 
-            sent(ref, sem, cond)
+            if (w, yy) == (1, 1):
+                sent(up_all.at[pl.ds(0, 4)], sem, cond)
             parts.append((cond, go))
         return parts
 
@@ -193,7 +192,7 @@
 
         @pl.when(cond)
         def _():
-            recv(alls[w].at[piece], wsend.at[w, piece], wrecv.at[w, piece])
+            recv(alls[w].at[piece], wsend.at[0, 0], wrecv.at[w, piece])
 
     def angles(b):
         at = sp * nblk + b
@@ -306,7 +305,7 @@
 
     def part_up(part):
         ref = up_all.at[other, pl.ds(part * hr, hr)]
-        rcopy(ref, ref, zsem(0, other, 0), wrecv.at[0, other], to_zp).start()
+        rcopy(ref, ref, wsend.at[0, 0], wrecv.at[0, other], to_zp).start()
 
     @pl.when(late)
     def _():
@@ -329,7 +328,6 @@
 
     def chain_end():
         rcopy(csend, crecv, ssend.at[1], srecv.at[0], to_zp).wait_send()
-        rcopy(up_all.at[other], up_all.at[other], zsem(0, other, 0), wrecv.at[0, other], to_zp).wait_send()
 
     pending.append((has_up, chain_end))
     for h in range(heads):
@@ -444,7 +442,7 @@
         own = x_all.at[c, y, x, at]
         send(own, own, asend.at[0, 0], ary.at[0, r], to_y, track=False)
         for j in range(1, X):
-            send(own, own, asend.at[1, j], arx.at[j, r], to_x(j), track=False)
+            send(own, own, asend.at[1, j], arx.at[j - 1, r], to_x(j), track=False)
         send(own, own, asend.at[2, 0], ard.at[0, 0], to_c, track=False)
 
     load(5).wait()
@@ -490,7 +488,7 @@
         if yrel:
             recv(ref, asend.at[0, 0], ary.at[i, r])
         else:
-            recv(ref, asend.at[1, i], arx.at[i, r])
+            recv(ref, asend.at[1, i], arx.at[i - 1, r])
             send(ref, ref, asend.at[0, i], ary.at[i, r], to_y, track=False)
         send(ref, ref, asend.at[2 + yrel, i], ard.at[yrel, i], to_c, track=False)
 
@@ -574,7 +572,7 @@
             @pl.when(jnp.logical_not(has_up & has_dn))
             def _():
                 ref = dn_all.at[self.block, pl.ds(r0, nr), pl.ds(c0, cw)]
-                recv(ref, wsend.at[1, 0], wlast.at[i])
+                recv(ref, wsend.at[0, 0], wlast.at[i])
 
         def product(self, cls, r0, nr):
             w = dn_all[self.block, r0 : r0 + nr, self.c0 : self.c0 + self.w]
@@ -593,16 +591,13 @@
             pd[self.t % 2, :, :, :, :, : self.w] = value.astype(BF16).reshape(2, X, 2, hm, self.w)
             self.to_sib().start()
 
-        def early(self):
+        def compute_late(self, before):
             self.arrive(1)
             ret[: 2 * X * mine, cw : 2 * cw] = self.product(1 - c, 0, ka)
-            ret[: 2 * X * mine, 2 * cw : 3 * cw] = self.product(c, 0, ka)
-
-        def late(self, before):
+            before()
             self.arrive(2)
-            before()
             self.offer(ret[: 2 * X * mine, cw : 2 * cw] + self.product(1 - c, ka, half - ka))
-            ret[: 2 * X * mine, :cw] = ret[: 2 * X * mine, 2 * cw : 3 * cw] + self.product(c, ka, half - ka)
+            ret[: 2 * X * mine, :cw] = self.product(c, 0, half)
 
         def first(self):
             k, at = self.t % SLOTS, slice(self.c0, self.c0 + self.w)
@@ -621,13 +616,8 @@
             qs[k, :, x, 1, :, :w] = s.astype(BF16)
             self.copies(1)
 
-        def put(self):
-            at = pl.ds(pl.multiple_of(self.block * cols + self.c0, 128), self.w)
-            return pltpu.make_async_copy(self.trim(out.at[self.t % 4], 0), out_h.at[:, at], osem.at[self.t % 4])
-
         def final(self):
             k, at, w = self.t % SLOTS, slice(self.c0, self.c0 + self.w), self.w
-            o = self.t % 4
             col = pl.ds(pl.multiple_of(self.block * cols + self.c0, 128), w)
             if self.part is not None:
                 every = (2 * X - 1) * 2
@@ -635,18 +625,16 @@
                 s = qs[k, y, x, :, :, :w].astype(F32)
                 for i in range(1, 2 * X):
                     s = s + rd[self.part, i].astype(F32)
-                out[o, :, :w] = (upd[:, col].astype(F32) + s.reshape(mine, w)).astype(BF16)
-                self.put().start()
+                out[:, col] = (upd[:, col].astype(F32) + s.reshape(mine, w)).astype(BF16)
                 self.bulk(every, qsem.at[0, k], qrecv.at[0, 0]).wait_send()
                 return
             self.bulk(nb, qsem.at[1, 0], qrecv.at[1, self.t]).wait_recv()
             s = upd[:hm, col].astype(F32) + qs[k, y, x, 0, :, :w].astype(F32)
             for j in range(1, X):
                 s = s + r3x[self.u, j - 1, :, at].astype(F32)
-            out[o, :hm, :w] = s.astype(BF16)
+            out[:hm, col] = s.astype(BF16)
             s = upd[hm:, col].astype(F32) + qs[k, y, x, 1, :, :w].astype(F32) + r3y[self.u, :, at].astype(F32)
-            out[o, hm:, :w] = s.astype(BF16)
-            self.put().start()
+            out[hm:, col] = s.astype(BF16)
             self.bulk(na, qsem.at[0, k], qrecv.at[0, 0]).wait_send()
             self.bulk(nb, qsem.at[1, k], qrecv.at[1, 0]).wait_send()
 
@@ -666,7 +654,6 @@
 
         @pl.when(s >= 4)
         def _():
-            pl.when(s >= 8)(lambda: Unit(s - 8).put().wait())
             Unit(s - 4).final()
 
         return carry
@@ -675,8 +662,6 @@
     tail = [Unit(t) for t in range(units)]
 
     def finish_unit(t):
-        if t >= 4:
-            tail[t - 4].put().wait()
         tail[t].final()
 
     if halves:
@@ -684,10 +669,9 @@
         one, two = tail[units], tail[units + 1]
         one.compute(tail[units - 2].wait_sib)
         tail[units - 2].second()
-        two.early()
         one.first()
         finish_unit(units - 4)
-        two.late(tail[units - 1].wait_sib)
+        two.compute_late(tail[units - 1].wait_sib)
         tail[units - 1].second()
         two.first()
         finish_unit(units - 3)
@@ -696,8 +680,6 @@
         tail[units - 1].second()
     for t in range(total - 4, total):
         finish_unit(t)
-    for t in range(total - 4, total):
-        tail[t].put().wait()
     for t in range(total - 2, total):
         tail[t].wait_sib()
     for cond, end in pending:
@@ -722,7 +704,7 @@
     hd, hv = heads * DK, heads * DV
     sq = (DK, DV // 2)
     scratch = [
-        V((heads, rows), F32), *[V(t.shape, F32) for t in tables], V((4, mine, cols), BF16),
+        V((heads, rows), F32), *[V(t.shape, F32) for t in tables],
         V((rows, hd), BF16), V((rows, hd), BF16), V((rows, hv), BF16), V((rows, hv), BF16),
         V((2 * X * mine, 2 * half), BF16), V((mine, d), BF16),
         V((heads, rows, DK), BF16), V((rows, DK), BF16),
@@ -738,19 +720,19 @@
         V((n_sp, X, mine // 2, cols), BF16), V((n_sp, X - 1, 2, mine // 2, cols), BF16),
         V((n_sp, mine // 2, cols), BF16), V((n_sp, X - 1, mine // 2, cols), BF16),
         V((2, 2 * X, 2, mine // 2, cols // 2), BF16),
-        dma((10 + 2 * X * mine // hv,)), dma((2, n_sp + 2)), dma((2, n_sp)), dma((3,)), dma((2,)), dma((2,)),
+        dma((10 + 2 * X * mine // hv,)), dma((2, max(1, n_sp // 2 - 1))), dma((2, n_sp)), dma((3,)), dma((2,)), dma((2,)),
         dma((4,)), dma((3 + heads,)), dma((X,)), dma((X, 2)), dma((X - 1,)), dma((X - 1, ROWS)),
-        dma((4, X)), dma((X, ROWS)), dma((X, ROWS)), dma((2, X)),
-        dma((2,)), dma((n_sp + 1,)), dma((2, SLOTS)), dma((2, n_sp + 1)), dma((4,)),
+        dma((4, X)), dma((X - 1, ROWS)), dma((X, ROWS)), dma((2, X)),
+        dma((2,)), dma((n_sp + 1,)), dma((2, SLOTS)), dma((2, n_sp + 1)),
     ]
     return pl.pallas_call(
         functools.partial(kernel, n_sp, n_tp),
         in_specs=[anym] * 7 + [vm] + [anym] * 4,
-        out_specs=anym,
-        out_shape=jax.ShapeDtypeStruct((mine, d), BF16),
+        out_specs=vm,
+        out_shape=pltpu.VMEM((mine, d), BF16),
         scratch_shapes=scratch,
         compiler_params=pltpu.CompilerParams(
-            collective_id=0, has_side_effects=True, vmem_limit_bytes=67043328
+            collective_id=0, has_side_effects=True, vmem_limit_bytes=62 * 2**20
         ),
         name="layer",
     )(resid, queries, keys, values, gates, log_decay, w_out, gain, up, down, *tables)

time: 158 us -> 155 us (0.981)
  no operation moved by 1% of the time
where the time goes in v4:
time: 155 us
  Pallas kernels  154 us (99%)
    pallas_call x1, Pallas kernels, body(): pl.pallas_call(functools.partial(kernel, n_sp, n_tp), in_specs=[anym] * 7...  154 us

profile of v4, /device:TPU:24, one launch (start us, length us, event | category | flops | bytes accessed | tf_op | source)
XLA Modules:
  0.0 155.3 jit_solution(7963239488314659327)
XLA Ops:
  0.0 154.3 %layer.1 = bf16[256,2048]{1,0:T(8,128)(2,1)S(1)} custom-call(bf16[256,2048]{1,0:T(8,128)(2,1)} %resid_h.1, bf16[1024,512]{1,0:T(8,128)(2,1)} %q_h.1, bf16[1024,512]{1,0:T(8,128)(2,1)} %k_h.1, bf16[1024,1024]{1,0:T(8,128)(2,1)} %v_h.1, bf16[1024,1024]{1,0:T(8,128)(2,1)} %g_h.1, f32[2,1024]{1,0:T(2,128)} %ld_h.1, bf16[1024,2048]{1,0:T(8,128)(2,1)} %wo_h.1, ...), custom_call_target="tpu_custom_call" | custom-call | tf_op jit(solution)/shard_map/layer/pallas_call | solution.py:728
  154.4 1.0 copy.14

commit v5 on v4

--- a/solution.py
+++ b/solution.py
@@ -58,7 +58,7 @@
     rc = mine // ROWS
     has_up, has_dn = z < Z - 1, z > 0
     halves = cols % 256 == 0 and Z > 2
-    cw, ka = cols // 2, half - min(256, half // 2)
+    cw, ka = cols // 2, half // 2
     pieces = ((0, half, 0), (0, ka, cw), (ka, half - ka, cw))
 
     def rcopy(src, dst, ss, rs, dev):
@@ -592,12 +592,14 @@
             self.to_sib().start()
 
         def compute_late(self, before):
+            near = slice(cw, 2 * cw), slice(2 * cw, 3 * cw)
             self.arrive(1)
-            ret[: 2 * X * mine, cw : 2 * cw] = self.product(1 - c, 0, ka)
+            ret[: 2 * X * mine, near[0]] = self.product(1 - c, 0, ka)
+            ret[: 2 * X * mine, near[1]] = self.product(c, 0, ka)
             before()
             self.arrive(2)
-            self.offer(ret[: 2 * X * mine, cw : 2 * cw] + self.product(1 - c, ka, half - ka))
-            ret[: 2 * X * mine, :cw] = self.product(c, 0, half)
+            self.offer(ret[: 2 * X * mine, near[0]] + self.product(1 - c, ka, half - ka))
+            ret[: 2 * X * mine, :cw] = ret[: 2 * X * mine, near[1]] + self.product(c, ka, half - ka)
 
         def first(self):
             k, at = self.t % SLOTS, slice(self.c0, self.c0 + self.w)

time: 155 us -> 155 us (level)
  no operation moved by 1% of the time
where the time goes in v5:
time: 155 us
  Pallas kernels  154 us (99%)
    pallas_call x1, Pallas kernels, body(): pl.pallas_call(functools.partial(kernel, n_sp, n_tp), in_specs=[anym] * 7...  154 us

profile of v5, /device:TPU:24, one launch (start us, length us, event | category | flops | bytes accessed | tf_op | source)
XLA Modules:
  0.0 155.3 jit_solution(15283083484132874603)
XLA Ops:
  0.0 154.3 %layer.1 = bf16[256,2048]{1,0:T(8,128)(2,1)S(1)} custom-call(bf16[256,2048]{1,0:T(8,128)(2,1)} %resid_h.1, bf16[1024,512]{1,0:T(8,128)(2,1)} %q_h.1, bf16[1024,512]{1,0:T(8,128)(2,1)} %k_h.1, bf16[1024,1024]{1,0:T(8,128)(2,1)} %v_h.1, bf16[1024,1024]{1,0:T(8,128)(2,1)} %g_h.1, f32[2,1024]{1,0:T(2,128)} %ld_h.1, bf16[1024,2048]{1,0:T(8,128)(2,1)} %wo_h.1, ...), custom_call_target="tpu_custom_call" | custom-call | tf_op jit(solution)/shard_map/layer/pallas_call | solution.py:730
  154.4 1.0 copy.14
